TPU v7x, 32 devices: a whole 2x2x4 slice. The times are simulated.
32 devices in a mesh: kv: 16 (over z, y, x), tp: 2 (over core).
Axes of the slice: x: 2, y: 2, z: 4, core: 2. Of those that a mesh axis runs over, the one named last changes fastest.
Arguments:
- tokens: bfloat16 [4096, 2048], P('kv'), may hold values from -72 to 72
- w_query: bfloat16 [2048, 1024], P(None, 'tp'), may hold values from -0.125 to 0.125
- w_key: bfloat16 [2048, 1024], P(None, 'tp'), may hold values from -0.125 to 0.125
- w_value: bfloat16 [2048, 1024], P(None, 'tp'), may hold values from -0.125 to 0.125
- w_out: bfloat16 [1024, 2048], P('tp'), may hold values from -0.1875 to 0.1875
- chosen: int32 [64, 16], replicated, may hold values from -1 to 63, as said below
Outputs:
- mixed: bfloat16 [4096, 2048], P(('kv', 'tp'))
- log_sums: float32 [16, 4096], P('tp', 'kv')
Inputs may be any that keep to these rules, and one draw needn't show every extreme that they name: `chosen`: row b begins with b itself, then lists distinct key blocks at most b, then holds -1 in its remaining entries. Taken together, the rows of the query blocks of one index of kv list at most 2 distinct blocks of the positions of any other index of kv, and exactly 2 for some pairs of indices in every draw.
All inputs are finite; a program needn't handle non-finite values.
Results may differ from a plain program's by a relative error of at most 0.03.
Values may be sent and summed in bfloat16 or wider, within the bound.
A program may use at most 64 MiB of HBM per device.

v0:
```python
import functools

import jax
import jax.numpy as jnp
from jax import lax
from jax.experimental import pallas as pl
from jax.experimental.pallas import tpu as pltpu
from jax.sharding import PartitionSpec as P

HEAD_DIM = 64
BLK = 64
CAP = 2
LANES = 128
VMEM_LIMIT = 48 * 1024 * 1024

rotary_base = 500000.0
masked_score = -1e30


def in_vmem():
    return pl.BlockSpec(memory_space=pltpu.VMEM)


def in_smem():
    return pl.BlockSpec(memory_space=pltpu.SMEM)


def attention_kernel(
    layers, group, blocks, places_ref, sel_ref, x_ref, wk_ref, wv_ref, wq_ref, cos_ref, sin_ref,
    out_ref, log_ref, wkv, wq, query, stage, picked, load_sem, col_send, col_recv, pl_send, pl_recv, *tables
):
    pairs = len(tables)
    entries = places_ref.shape[1] - 1
    me = lax.axis_index("kv")
    z = lax.div(me, group)
    g = lax.rem(me, group)
    up = lax.rem(me + group, layers * group)
    down = lax.rem(me + (layers - 1) * group, layers * group)
    half = HEAD_DIM // 2
    mesh_ids = pl.DeviceIdType.MESH
    peers = [z * group + lax.rem(g + d, group) for d in range(group)]

    def load(kind, ch):
        lanes = pl.ds(ch * LANES, LANES)
        source = (wk_ref, wv_ref, wq_ref)[kind].at[:, lanes]
        if kind < 2:
            target = wkv.at[ch, :, pl.ds(kind * LANES, LANES)]
        else:
            target = wq.at[:, lanes]
        return pltpu.make_async_copy(source, target, load_sem.at[kind, ch])

    for ch in range(pairs):
        load(0, ch).start()
        load(1, ch).start()
    for ch in range(pairs):
        load(2, ch).start()

    barrier = pltpu.get_barrier_semaphore()
    for d in range(1, group):
        pl.semaphore_signal(barrier, inc=1, device_id={"kv": peers[d]}, device_id_type=mesh_ids)

    @pl.when(z < layers - 1)
    def _():
        pl.semaphore_signal(barrier, inc=1, device_id={"kv": up}, device_id_type=mesh_ids)

    @pl.when(z > 0)
    def _():
        pl.semaphore_signal(barrier, inc=1, device_id={"kv": down}, device_id_type=mesh_ids)

    def column_copy(t, ch):
        return pltpu.make_async_remote_copy(
            src_ref=tables[ch].at[pl.ds(t * blocks, blocks)],
            dst_ref=tables[ch].at[pl.ds((t + 1) * blocks, blocks)],
            send_sem=col_send.at[t, ch],
            recv_sem=col_recv.at[t, ch],
            device_id={"kv": up},
            device_id_type=mesh_ids,
        )

    def plane_copy(d, t, ch):
        place = layers * blocks + ((d - 1) * layers + t) * CAP
        return pltpu.make_async_remote_copy(
            src_ref=stage.at[d - 1, t, ch],
            dst_ref=tables[ch].at[pl.ds(place, CAP)],
            send_sem=pl_send.at[d - 1, t, ch],
            recv_sem=pl_recv.at[d - 1, t, ch],
            device_id={"kv": peers[d]},
            device_id_type=mesh_ids,
        )

    def hand_on(d, t, ch):
        for c in range(CAP):
            index = sel_ref[peers[d], ((z - t) * group + g) * CAP + c]
            chosen_tile = None
            for i in range(blocks):
                tile = tables[ch][t * blocks + i]
                chosen_tile = tile if chosen_tile is None else jnp.where(index == i, tile, chosen_tile)
            stage[d - 1, t, ch, c] = chosen_tile
        plane_copy(d, t, ch).start()

    def send_set(t, ch):
        if t < layers - 1:

            @pl.when(z < layers - 1)
            def _():
                column_copy(t, ch).start()

        for d in range(1, group):
            if t == 0:
                pl.when(g + d < group)(functools.partial(hand_on, d, t, ch))
            else:
                hand_on(d, t, ch)

    cos_part = cos_ref[...]
    sin_part = sin_ref[...]
    low = lax.broadcasted_iota(jnp.int32, cos_part.shape, 1) % HEAD_DIM < half

    def turned(part):
        other = jnp.where(low, pltpu.roll(part, LANES - half, 1), pltpu.roll(part, half, 1))
        return part * cos_part + other * sin_part

    for ch in range(pairs):
        load(0, ch).wait()
        load(1, ch).wait()
        made = jnp.dot(x_ref[...], wkv[ch], preferred_element_type=jnp.float32)
        key_rows = turned(made[:, :LANES]).astype(jnp.bfloat16)
        value_rows = made[:, LANES:].astype(jnp.bfloat16)
        for i in range(blocks):
            tables[ch][i, :, :LANES] = key_rows[i * BLK : (i + 1) * BLK]
            tables[ch][i, :, LANES:] = value_rows[i * BLK : (i + 1) * BLK]
        if ch == 0:
            pl.semaphore_wait(barrier, group - 1 + jnp.minimum(z, 1) + jnp.minimum(layers - 1 - z, 1))
        send_set(0, ch)

    for ch in range(pairs):
        load(2, ch).wait()
    wide = min(2 * LANES, pairs * LANES)
    for lane in range(0, pairs * LANES, wide):
        made = jnp.dot(x_ref[...], wq[:, lane : lane + wide], preferred_element_type=jnp.float32)
        for part in range(0, wide, LANES):
            piece = turned(made[:, part : part + LANES]).astype(jnp.bfloat16)
            query[:, lane + part : lane + part + LANES] = (piece * (HEAD_DIM**-0.5)).astype(jnp.bfloat16)

    first = lax.broadcasted_iota(jnp.int32, (BLK, LANES), 1) < HEAD_DIM
    lane_index = lax.broadcasted_iota(jnp.int32, (BLK, LANES), 1)

    def attend(ch):
        lanes = slice(ch * LANES, (ch + 1) * LANES)

        def one_block(r, carry):
            count = places_ref[r, entries]
            for s in range(entries):
                picked[s * BLK : (s + 1) * BLK, :] = tables[ch][places_ref[r, s]]
            rows = pl.ds(pl.multiple_of(r * BLK, BLK), BLK)
            live = lax.broadcasted_iota(jnp.int32, (2 * BLK, entries * BLK), 1) < count * BLK
            both = query[rows, lanes]
            none = jnp.zeros_like(both)
            stacked = jnp.concatenate([jnp.where(first, both, none), jnp.where(first, none, both)], axis=0)
            scores = lax.dot_general(
                stacked, picked[:, :LANES], (((1,), (1,)), ((), ())), preferred_element_type=jnp.float32
            )
            scores = jnp.where(live, scores, masked_score)
            top = jnp.max(scores, axis=1, keepdims=True)
            weights = jnp.exp(scores - top)
            total = jnp.sum(weights, axis=1, keepdims=True)
            summed = jnp.dot(
                weights.astype(jnp.bfloat16), picked[:, LANES:], preferred_element_type=jnp.float32
            )
            summed = summed / total
            out_ref[rows, lanes] = jnp.where(first, summed[:BLK], summed[BLK:]).astype(jnp.bfloat16)
            log_sum = top + jnp.log(total)
            logs = jnp.zeros((BLK, LANES), jnp.float32) if ch == 0 else log_ref[rows, :]
            logs = jnp.where(lane_index == 2 * ch, log_sum[:BLK], logs)
            log_ref[rows, :] = jnp.where(lane_index == 2 * ch + 1, log_sum[BLK:], logs)
            return carry

        lax.fori_loop(0, blocks, one_block, 0)

    def finish(ch):
        for t in range(layers):

            @pl.when(z >= t)
            def _():
                for d in range(1, group):
                    if t == 0:
                        pl.when(g >= d)(lambda d=d: plane_copy(d, t, ch).wait_recv())
                    else:
                        plane_copy(d, t, ch).wait_recv()

        attend(ch)

    for ch in range(pairs):
        for t in range(1, layers):

            @pl.when(z >= t)
            def _():
                column_copy(t - 1, ch).wait_recv()
                send_set(t, ch)

        if ch > 0:
            finish(ch - 1)
    finish(pairs - 1)

    for ch in range(pairs):
        for t in range(layers):

            @pl.when(z >= t)
            def _():
                if t < layers - 1:

                    @pl.when(z < layers - 1)
                    def _():
                        column_copy(t, ch).wait_send()

                for d in range(1, group):
                    if t == 0:
                        pl.when(g + d < group)(lambda d=d: plane_copy(d, t, ch).wait_send())
                    else:
                        plane_copy(d, t, ch).wait_send()


def mix_kernel(n, att_ref, w_ref, out_ref, stage, landed, send_sem, recv_sem):
    me = lax.axis_index("tp")
    rows = out_ref.shape[0]
    tile = min(512, w_ref.shape[1])
    tiles = w_ref.shape[1] // tile
    peers = [lax.rem(me + d, n) for d in range(n)]
    barrier = pltpu.get_barrier_semaphore()
    for d in range(1, n):
        pl.semaphore_signal(barrier, inc=1, device_id={"tp": peers[d]}, device_id_type=pl.DeviceIdType.MESH)
    pl.semaphore_wait(barrier, n - 1)

    def partial_of(d, j):
        mine = att_ref[pl.ds(pl.multiple_of(peers[d] * rows, rows), rows), :]
        made = jnp.dot(mine, w_ref[:, j * tile : (j + 1) * tile], preferred_element_type=jnp.float32)
        return made.astype(jnp.bfloat16)

    def hop(d, j):
        return pltpu.make_async_remote_copy(
            src_ref=stage.at[d - 1, j],
            dst_ref=landed.at[d - 1, j],
            send_sem=send_sem.at[d - 1, j],
            recv_sem=recv_sem.at[d - 1, j],
            device_id={"tp": peers[d]},
            device_id_type=pl.DeviceIdType.MESH,
        )

    for d in range(1, n):
        for j in range(tiles):
            stage[d - 1, j] = partial_of(d, j)
            hop(d, j).start()
    for j in range(tiles):
        acc = partial_of(0, j).astype(jnp.float32)
        for d in range(1, n):
            hop(d, j).wait_recv()
            acc = acc + landed[d - 1, j].astype(jnp.float32)
        out_ref[:, j * tile : (j + 1) * tile] = acc.astype(jnp.bfloat16)
    for d in range(1, n):
        for j in range(tiles):
            hop(d, j).wait_send()


def local(devices, splits, tokens, w_query, w_key, w_value, w_out, chosen):
    rows, depth = tokens.shape
    width = w_query.shape[1]
    heads = width // HEAD_DIM
    blocks = rows // BLK
    group = 1
    while group * group < devices:
        group *= 2
    layers = devices // group
    all_blocks = chosen.shape[0]
    me = lax.axis_index("kv")

    half = HEAD_DIM // 2
    inverse = rotary_base ** (-jnp.arange(half, dtype=jnp.float32) / half)
    positions = (me * rows + jnp.arange(rows)).astype(jnp.float32)
    angles = positions[:, None] * inverse[None, :]
    cos_half, sin_half = jnp.cos(angles), jnp.sin(angles)
    cos_part = jnp.concatenate([cos_half] * (LANES // half), axis=1)
    sin_part = jnp.concatenate([-sin_half, sin_half] * (LANES // HEAD_DIM), axis=1)

    flat = chosen.reshape(devices, -1)
    listed = jnp.any(flat[:, :, None] == jnp.arange(all_blocks)[None, None, :], axis=1)
    listed = listed.reshape(devices, devices, blocks).astype(jnp.int32)
    before = (jnp.arange(blocks)[:, None] < jnp.arange(blocks)[None, :]).astype(jnp.int32)
    slots = jnp.sum(listed[:, :, :, None] * before[None, None], axis=2)
    fits = (slots[:, :, None, :] == jnp.arange(CAP)[:, None]) & (listed[:, :, None, :] > 0)
    sel = jnp.sum(jnp.where(fits, jnp.arange(blocks), 0), axis=-1).reshape(devices, devices * CAP)

    own_lists = lax.dynamic_slice_in_dim(chosen, me * blocks, blocks, 0)
    own_slots = lax.dynamic_slice_in_dim(slots.reshape(devices, all_blocks), me, 1, 0)
    own_blocks = jnp.where(own_lists >= 0, own_lists, me * blocks + jnp.arange(blocks)[:, None])
    every_block = jnp.arange(all_blocks)
    owners = every_block // blocks
    steps = me // group - owners // group
    across = (me % group - owners % group + group) % group
    handed = layers * blocks + ((across - 1) * layers + steps) * CAP + jnp.minimum(own_slots[0], CAP - 1)
    home = jnp.where(across == 0, steps * blocks + every_block % blocks, handed)
    places = jnp.sum(jnp.where(own_blocks[:, :, None] == every_block, home, 0), axis=-1)
    counts = jnp.sum((own_lists >= 0).astype(jnp.int32), axis=1, keepdims=True)
    places = jnp.concatenate([places, counts], axis=1)

    table_blocks = layers * blocks + (group - 1) * layers * CAP
    pairs = width // LANES
    in_hbm = pl.BlockSpec(memory_space=pltpu.HBM)
    attended, logs = pl.pallas_call(
        functools.partial(attention_kernel, layers, group, blocks),
        in_specs=[in_smem()] * 2 + [in_vmem()] + [in_hbm] * 3 + [in_vmem()] * 2,
        out_specs=[in_vmem(), in_vmem()],
        out_shape=[
            jax.ShapeDtypeStruct((rows, width), jnp.bfloat16),
            jax.ShapeDtypeStruct((rows, LANES), jnp.float32),
        ],
        scratch_shapes=[
            pltpu.VMEM((pairs, depth, 2 * LANES), jnp.bfloat16),
            pltpu.VMEM((depth, width), jnp.bfloat16),
            pltpu.VMEM((rows, width), jnp.bfloat16),
            pltpu.VMEM((group - 1, layers, pairs, CAP, BLK, 2 * LANES), jnp.bfloat16),
            pltpu.VMEM((chosen.shape[1] * BLK, 2 * LANES), jnp.bfloat16),
            pltpu.SemaphoreType.DMA((3, pairs)),
            pltpu.SemaphoreType.DMA((layers, pairs)),
            pltpu.SemaphoreType.DMA((layers, pairs)),
            pltpu.SemaphoreType.DMA((group - 1, layers, pairs)),
            pltpu.SemaphoreType.DMA((group - 1, layers, pairs)),
        ]
        + [pltpu.VMEM((table_blocks, BLK, 2 * LANES), jnp.bfloat16)] * pairs,
        compiler_params=pltpu.CompilerParams(
            collective_id=0, has_side_effects=True, vmem_limit_bytes=VMEM_LIMIT
        ),
        name="attention",
    )(places, sel, tokens, w_key, w_value, w_query, cos_part, sin_part)
    log_sums = jnp.transpose(logs[:, :heads])

    out_rows = rows // splits
    tile = min(512, w_out.shape[1])
    out_tiles = w_out.shape[1] // tile
    output = pl.pallas_call(
        functools.partial(mix_kernel, splits),
        in_specs=[in_vmem(), in_vmem()],
        out_specs=in_vmem(),
        out_shape=jax.ShapeDtypeStruct((out_rows, w_out.shape[1]), jnp.bfloat16),
        scratch_shapes=[
            pltpu.VMEM((splits - 1, out_tiles, out_rows, tile), jnp.bfloat16),
            pltpu.VMEM((splits - 1, out_tiles, out_rows, tile), jnp.bfloat16),
            pltpu.SemaphoreType.DMA((splits - 1, out_tiles)),
            pltpu.SemaphoreType.DMA((splits - 1, out_tiles)),
        ],
        compiler_params=pltpu.CompilerParams(
            collective_id=1, has_side_effects=True, vmem_limit_bytes=VMEM_LIMIT
        ),
        name="mix",
    )(attended, w_out)
    return (output, log_sums)


def solution(mesh):
    placed = (P("kv", None), P(None, "tp"), P(None, "tp"), P(None, "tp"), P("tp", None), P())
    return jax.shard_map(
        functools.partial(local, mesh.shape["kv"], mesh.shape["tp"]),
        mesh=mesh,
        in_specs=placed,
        out_specs=(P(("kv", "tp"), None), P("tp", "kv")),
        check_vma=False,
    )
```

profile of v0, /device:TPU:25, one launch (start us, length us, event | category | flops | bytes accessed | tf_op | source)
XLA Modules:
  0.0 66.5 jit_solution(11029460809448338800)
XLA Ops:
  0.7 0.9 %compare_select_fusion = (s32[4,16]{0,1:T(8,128)S(1)}, s32[4]{0:T(128)S(1)}) fusion(s32[64,16]{0,1:T(8,128)} %param.11, s32[]{:T(128)S(6)} %select_n.56, s32[4]{0:T(128)S(1)} %iota_add_fusion), kind=kLoop, calls=%fused_computation.17 | loop fusion | flops 252 | bytes 548 | tf_op jit(solution)/shard_map/jit(_where)/select_n | solution.py:293
  1.6 0.1 copy.37
  1.7 0.1 copy.42
  1.7 0.8 %copy.38 = s32[64,16]{1,0:T(8,128)S(1)} copy(s32[64,16]{0,1:T(8,128)} %param.11) | data formatting | bytes 8192 | tf_op args[5]
  2.5 0.1 eq.55
  2.6 0.2 fusion
  2.8 0.1 copy.39
  3.0 0.1 copy.40
  3.0 0.1 multiply_reduce_fusion
  3.1 0.1 copy.43
  3.2 0.1 copy.41
  3.3 0.2 minimum_reduce_fusion
  3.5 0.2 select_reduce_fusion.1
  3.8 0.1 pad_add_fusion.places_ref
  3.8 0.1 copy.44
  3.9 0.1 copy.46.sel_ref
  4.0 0.5 fusion.2
  4.5 0.3 pad_maximum_fusion
  4.8 1.6 %copy-done = bf16[2048,512]{1,0:T(8,128)(2,1)S(1)} copy-done((bf16[2048,512]{1,0:T(8,128)(2,1)S(1)}, bf16[2048,512]{1,0:T(8,128)(2,1)}, u32[]{:S(2)}) %copy-start) | copy-done | bytes 2097176
  6.4 1.6 %copy-done.1 = bf16[2048,512]{1,0:T(8,128)(2,1)S(1)} copy-done((bf16[2048,512]{1,0:T(8,128)(2,1)S(1)}, bf16[2048,512]{1,0:T(8,128)(2,1)}, u32[]{:S(2)}) %copy-start.1) | copy-done | bytes 2097176
  8.0 50.2 %attention.1 = (bf16[256,512]{1,0:T(8,128)(2,1)S(1)}, f32[256,128]{1,0:T(8,128)S(1)}) custom-call(s32[4,17]{1,0:T(4,128)S(1)} %pad_add_fusion.places_ref, s32[16,32]{1,0:T(8,128)S(1)} %copy.46.sel_ref, bf16[256,2048]{1,0:T(8,128)(2,1)S(1)} %copy-done.3, bf16[2048,512]{1,0:T(8,128)(2,1)S(1)} %copy-done, bf16[2048,512]{1,0:T(8,128)(2,1)S(1)} %copy-done.1, ...), custom_call_target="tpu_custom_call" | custom-call | tf_op jit(solution)/shard_map/attention/pallas_call | solution.py:307
  58.2 0.7 %copy.47 = f32[8,256]{1,0:T(8,128)} copy(f32[8,256]{0,1:T(8,128)S(1)} %slice_bitcast_fusion) | data formatting | bytes 16384
  58.9 6.8 %mix.1 = bf16[128,2048]{1,0:T(8,128)(2,1)S(1)} custom-call(bf16[256,512]{1,0:T(8,128)(2,1)S(1)} %get-tuple-element.4.att_ref, bf16[512,2048]{1,0:T(8,128)(2,1)S(1)} %copy-done.2), custom_call_target="tpu_custom_call" | custom-call | tf_op jit(solution)/shard_map/mix/pallas_call | solution.py:338
  65.7 0.8 %copy.49 = bf16[128,2048]{1,0:T(8,128)(2,1)} copy(bf16[128,2048]{1,0:T(8,128)(2,1)S(1)} %mix.1) | data formatting | bytes 1048576
  (15 shorter events, 0.1 us)
Async XLA Ops:
  0.6 4.2 %copy-start.3 = (bf16[256,2048]{1,0:T(8,128)(2,1)S(1)}, bf16[256,2048]{1,0:T(8,128)(2,1)}, u32[]{:S(2)}) copy-start(bf16[256,2048]{1,0:T(8,128)(2,1)} %x_ref.1) | copy-start | bytes 3145732
  4.8 1.6 %copy-start = (bf16[2048,512]{1,0:T(8,128)(2,1)S(1)}, bf16[2048,512]{1,0:T(8,128)(2,1)}, u32[]{:S(2)}) copy-start(bf16[2048,512]{1,0:T(8,128)(2,1)} %wk_ref.1) | copy-start | bytes 6291460
  6.4 1.6 %copy-start.1 = (bf16[2048,512]{1,0:T(8,128)(2,1)S(1)}, bf16[2048,512]{1,0:T(8,128)(2,1)}, u32[]{:S(2)}) copy-start(bf16[2048,512]{1,0:T(8,128)(2,1)} %wv_ref.1) | copy-start | bytes 6291460
  8.0 50.9 %copy-start.2 = (bf16[512,2048]{1,0:T(8,128)(2,1)S(1)}, bf16[512,2048]{1,0:T(8,128)(2,1)}, u32[]{:S(2)}) copy-start(bf16[512,2048]{1,0:T(8,128)(2,1)} %w_ref.1) | copy-start | bytes 6291460
where the time goes:
time: 66.8 us; the launch traced here: 66.5 us
  Pallas kernels  57 us (85%)
  local copies, waits for them, and re-layouts  6.17 us (9%)
  other arithmetic  2.56 us (4%)
  between operations  0.78 us (1%)
    pallas_call x1, Pallas kernels, local(): pl.pallas_call(functools.partial(attention_kernel, layers, group, blocks)...  50.2 us
    pallas_call x1, Pallas kernels, local(): pl.pallas_call(functools.partial(mix_kernel, splits), in_specs=[in_vmem()...  6.83 us
    unnamed x11, local copies, waits for them, and re-layouts  5.43 us

commit v1 on v0

v1 whole, which is shorter than its diff:
```python
import functools

import jax
import jax.numpy as jnp
import numpy as np
from jax import lax
from jax.experimental import pallas as pl
from jax.experimental.pallas import tpu as pltpu
from jax.sharding import PartitionSpec as P

HEAD_DIM = 64
BLK = 64
LANES = 128
VMEM_LIMIT = 65_000_000

rotary_base = 500000.0
masked_score = -1e30

MESH = pl.DeviceIdType.MESH


def in_vmem():
    return pl.BlockSpec(memory_space=pltpu.VMEM)


def in_smem():
    return pl.BlockSpec(memory_space=pltpu.SMEM)


def in_hbm():
    return pl.BlockSpec(memory_space=pltpu.HBM)


def swap_halves(tile):
    return pltpu.roll(tile, LANES // 2, 1)


def layer_kernel(
    devices, splits, chosen_ref, x_ref, wq_ref, wk_ref, wv_ref, wo_ref, cos_ref, sin_ref, base_ref,
    mine_ref, landed_ref, log_ref,
    x, wq, wkv, wo, cos_t, sin_t, kv_out, q_out, kv_in, vk_in, q_in, o_out, l_out, o_in, l_in, weight, total_log,
    attended, stage, load_sem, kv_send, kv_recv, q_send, q_recv, o_send, o_recv, l_send, l_recv, tp_send, tp_recv,
):
    heads = kv_out.shape[0]
    pairs = heads // 2
    groups = devices // heads
    blocks = kv_out.shape[1]
    tiles = blocks // 2
    rows = blocks * BLK
    entries = chosen_ref.shape[0]
    table_blocks = heads * blocks
    wide = wq.shape[2] // LANES

    me = lax.axis_index("kv")
    tp = lax.axis_index("tp")
    group = lax.div(me, heads)
    idx = lax.rem(me, heads)
    first_device = group * heads
    half = HEAD_DIM // 2

    def pair_of(i):
        return lax.rem(lax.div(idx, 2) + 1 + i, pairs)

    def strip(ref, i):
        return ref.at[:, pl.ds(pl.multiple_of(pair_of(i) * LANES, LANES), LANES)]

    def load_q(i):
        target = wq.at[i // wide, :, pl.ds((i % wide) * LANES, LANES)]
        return pltpu.make_async_copy(strip(wq_ref, i), target, load_sem.at[0, i])

    def load_k(i):
        return pltpu.make_async_copy(strip(wk_ref, i), wkv.at[i, :, pl.ds(0, LANES)], load_sem.at[1, i])

    def load_v(i):
        return pltpu.make_async_copy(strip(wv_ref, i), wkv.at[i, :, pl.ds(LANES, LANES)], load_sem.at[2, i])

    load_x = pltpu.make_async_copy(x_ref, x, load_sem.at[3, 0])
    load_cos = pltpu.make_async_copy(cos_ref, cos_t, load_sem.at[4, 0])
    load_sin = pltpu.make_async_copy(sin_ref, sin_t, load_sem.at[5, 0])
    load_o = pltpu.make_async_copy(wo_ref, wo, load_sem.at[6, 0])

    load_x.start()
    load_cos.start()
    load_sin.start()
    for i in range(pairs):
        load_k(i).start()
        load_v(i).start()
        if i % wide == 0:
            for e in range(wide):
                load_q(i + e).start()
    load_o.start()

    barrier = pltpu.get_barrier_semaphore()

    def greet(d, carry):
        pl.semaphore_signal(
            barrier, inc=1, device_id={"kv": lax.rem(me + d, devices)}, device_id_type=MESH
        )
        return carry

    lax.fori_loop(1, devices, greet, 0)
    for d in range(1, splits):
        pl.semaphore_signal(barrier, inc=1, device_id={"tp": lax.rem(tp + d, splits)}, device_id_type=MESH)

    def kv_copy(slot, head):
        return pltpu.make_async_remote_copy(
            src_ref=kv_out.at[slot],
            dst_ref=kv_in.at[idx],
            send_sem=kv_send.at[head],
            recv_sem=kv_recv.at[idx],
            device_id={"kv": first_device + head},
            device_id_type=MESH,
        )

    def q_copy(slot, target):
        return pltpu.make_async_remote_copy(
            src_ref=q_out.at[slot],
            dst_ref=q_in.at[me],
            send_sem=q_send.at[target],
            recv_sem=q_recv.at[me],
            device_id={"kv": target},
            device_id_type=MESH,
        )

    def o_copy(target):
        return pltpu.make_async_remote_copy(
            src_ref=o_out.at[target],
            dst_ref=o_in.at[group, idx],
            send_sem=o_send.at[target],
            recv_sem=o_recv.at[me],
            device_id={"kv": target},
            device_id_type=MESH,
        )

    def l_copy(target):
        return pltpu.make_async_remote_copy(
            src_ref=l_out.at[target],
            dst_ref=l_in.at[group, idx],
            send_sem=l_send.at[target],
            recv_sem=l_recv.at[me],
            device_id={"kv": target},
            device_id_type=MESH,
        )

    def arrival(copy, semaphore):
        return pltpu.make_async_remote_copy(
            src_ref=copy, dst_ref=copy, send_sem=semaphore, recv_sem=semaphore,
            device_id={"kv": me}, device_id_type=MESH,
        )

    load_x.wait()
    load_cos.wait()
    load_sin.wait()
    low_rows = lax.broadcasted_iota(jnp.int32, (rows, LANES), 1) < LANES // 2
    turn_low = lax.broadcasted_iota(jnp.int32, (rows, LANES), 1) % HEAD_DIM < half
    cos_base = base_ref[0, pl.ds(me, 1), :]
    sin_base = base_ref[1, pl.ds(me, 1), :]
    cos_part = cos_t[...] * cos_base - sin_t[...] * sin_base
    sin_part = sin_t[...] * cos_base + cos_t[...] * sin_base
    sin_part = jnp.where(turn_low, -sin_part, sin_part)

    def turned(part):
        other = jnp.where(turn_low, pltpu.roll(part, LANES - half, 1), pltpu.roll(part, half, 1))
        return part * cos_part + other * sin_part

    def make_kv(i):
        load_k(i).wait()
        load_v(i).wait()
        made = jnp.dot(x[...], wkv[i], preferred_element_type=jnp.float32)
        keys = turned(made[:, :LANES])
        values = made[:, LANES:]
        even = jnp.where(low_rows, keys, swap_halves(values)).astype(jnp.bfloat16)
        odd = jnp.where(low_rows, swap_halves(keys), values).astype(jnp.bfloat16)
        for r in range(blocks):
            kv_out[2 * i, r] = even[r * BLK : (r + 1) * BLK]
            kv_out[2 * i + 1, r] = odd[r * BLK : (r + 1) * BLK]

    def make_q(i):
        for e in range(wide):
            load_q(i + e).wait()
        made = jnp.dot(x[...], wq[i // wide], preferred_element_type=jnp.float32)
        for e in range(wide):
            part = turned(made[:, e * LANES : (e + 1) * LANES]) * (HEAD_DIM**-0.5)
            swapped = swap_halves(part)
            low = low_rows[:BLK]
            for m in range(tiles):
                a = slice(2 * m * BLK, (2 * m + 1) * BLK)
                b = slice((2 * m + 1) * BLK, (2 * m + 2) * BLK)
                q_out[2 * (i + e), m] = jnp.where(low, part[a], swapped[b]).astype(jnp.bfloat16)
                q_out[2 * (i + e) + 1, m] = jnp.where(low, swapped[a], part[b]).astype(jnp.bfloat16)

    def send_kv(i):
        for e in range(2):
            head = 2 * pair_of(i) + e
            if i < pairs - 1:
                kv_copy(2 * i + e, head).start()
            else:
                pl.when(head != idx)(lambda e=e, head=head: kv_copy(2 * i + e, head).start())

    def send_q(i):
        for e in range(2):
            head = 2 * pair_of(i) + e
            if i < pairs - 1:
                q_copy(2 * i + e, first_device + head).start()
            else:
                pl.when(head != idx)(lambda e=e, head=head: q_copy(2 * i + e, first_device + head).start())

    for i in range(pairs):
        make_kv(i)
        if i == 0:
            pl.semaphore_wait(barrier, devices - 1 + splits - 1)
        send_kv(i)
        if i % wide == 0:
            make_q(i)
        send_q(i)

    def send_down(a, carry):
        for i in range(pairs):
            for e in range(2):
                q_copy(2 * i + e, a * heads + 2 * pair_of(i) + e).start()
        return carry

    lax.fori_loop(0, group, send_down, 0)

    own_slot = 2 * (pairs - 1) + lax.rem(idx, 2)
    for r in range(blocks):
        kv_in[idx, r] = kv_out[own_slot, r]
    for m in range(tiles):
        q_in[me, m] = q_out[own_slot, m]

    low = lax.broadcasted_iota(jnp.int32, (BLK, LANES), 1) < LANES // 2
    lane = lax.broadcasted_iota(jnp.int32, (BLK, LANES), 1)
    low_line = lax.broadcasted_iota(jnp.int32, (1, LANES), 1) < LANES // 2

    def take_kv(k, carry):
        source = lax.rem(idx + k, heads)

        @pl.when(k > 0)
        def _():
            arrival(kv_in.at[source], kv_recv.at[source]).wait_recv()

        for r in range(blocks):
            vk_in[source, r] = swap_halves(kv_in[source, r].astype(jnp.float32)).astype(jnp.bfloat16)
        return carry

    lax.fori_loop(0, heads, take_kv, 0)

    def attend(j):
        logs = jnp.zeros((BLK, LANES), jnp.float32)
        for m in range(tiles):
            tile = q_in[j, m]
            swapped = swap_halves(tile.astype(jnp.float32)).astype(jnp.bfloat16)
            none = jnp.zeros_like(tile)
            results = []
            for e in range(2):
                r = 2 * m + e
                at_low, at_high = (tile, swapped) if e == 0 else (swapped, tile)
                stacked = jnp.concatenate([jnp.where(low, at_low, none), jnp.where(low, none, at_high)], axis=0)
                bias, places = [], []
                for s in range(entries):
                    place = chosen_ref[s, j * blocks + r] - first_device * blocks
                    held = (place >= 0) & (place < table_blocks)
                    bias.append(jnp.where(held, 0.0, masked_score).astype(jnp.float32))
                    places.append(jnp.where(held, place, 0))
                scores, values = [], []
                for lower in range(0, entries, 8):
                    keys_here, values_here = [], []
                    for s in range(lower, lower + 8, 2):
                        a_place, b_place = places[s], places[s + 1]
                        a = kv_in[lax.div(a_place, blocks), lax.rem(a_place, blocks)]
                        b = vk_in[lax.div(b_place, blocks), lax.rem(b_place, blocks)]
                        keys_here.append(jnp.where(low, a, b))
                        values_here.append(jnp.where(low, b, a))
                    made = lax.dot_general(
                        stacked, jnp.concatenate(keys_here, axis=0), (((1,), (1,)), ((), ())),
                        preferred_element_type=jnp.float32,
                    )
                    lines = []
                    for first in range(2):
                        lines.append(
                            jnp.concatenate(
                                [
                                    jnp.where(low_line, bias[s + first], bias[s + 2 + first])
                                    for s in range(lower, lower + 8, 4)
                                ],
                                axis=1,
                            )
                        )
                    scores.append((made[:BLK] + lines[0], made[BLK:] + lines[1]))
                    values.append(jnp.concatenate(values_here, axis=0))
                top = functools.reduce(jnp.maximum, [part for both in scores for part in both])
                top = jnp.max(top, axis=1, keepdims=True)
                total = 0.0
                made = 0.0
                for both, held_values in zip(scores, values):
                    weights = [jnp.exp(part - top) for part in both]
                    total = total + weights[0] + weights[1]
                    rounded = jnp.concatenate([part.astype(jnp.bfloat16) for part in weights], axis=0)
                    made = made + jnp.dot(rounded, held_values, preferred_element_type=jnp.float32)
                total = jnp.sum(total, axis=1, keepdims=True)
                if e == 0:
                    summed = swap_halves(made[:BLK]) + made[BLK:]
                else:
                    summed = made[:BLK] + swap_halves(made[BLK:])
                results.append(summed / total)
                logs = jnp.where(lane == r, top + jnp.log(total), logs)
            o_out[j, m] = jnp.where(low, results[0], results[1]).astype(jnp.bfloat16)
        lines = jnp.transpose(jnp.concatenate([logs, jnp.zeros_like(logs)], axis=0))
        l_out[j] = lines[:8]

    def serve(t, carry):
        other_group = group + lax.div(t, heads)
        j = other_group * heads + lax.rem(idx + t, heads)

        @pl.when(t > 0)
        def _():
            arrival(q_in.at[j], q_recv.at[j]).wait_recv()

        attend(j)

        @pl.when(t > 0)
        def _():
            o_copy(j).start()
            l_copy(j).start()

        @pl.when(t == 0)
        def _():
            for m in range(tiles):
                o_in[group, idx, m] = o_out[j, m]
            l_in[group, idx] = l_out[j]

        return carry

    lax.fori_loop(0, devices - first_device, serve, 0)

    def absent(a, carry):
        o_in[a] = jnp.zeros(o_in.shape[1:], o_in.dtype)
        l_in[a] = jnp.full(l_in.shape[1:], masked_score, jnp.float32)
        return carry

    lax.fori_loop(group + 1, groups, absent, 0)

    def take_results(k, carry):
        source = lax.rem(me + k, (group + 1) * heads)
        place = o_in.at[lax.div(source, heads), lax.rem(source, heads)]
        arrival(place, o_recv.at[source]).wait_recv()
        line = l_in.at[lax.div(source, heads), lax.rem(source, heads)]
        arrival(line, l_recv.at[source]).wait_recv()
        return carry

    lax.fori_loop(1, (group + 1) * heads, take_results, 0)

    load_o.wait()

    def spread(body, start):
        if groups <= 2:
            for a in range(groups):
                start = body(a, start)
            return start
        return lax.fori_loop(0, groups, body, start)

    highest = spread(lambda a, top: jnp.maximum(top, l_in[a]), jnp.full(l_in.shape[1:], masked_score, jnp.float32))
    sums = spread(lambda a, acc: acc + jnp.exp(l_in[a] - highest), jnp.zeros(l_in.shape[1:], jnp.float32))
    total_log[...] = highest + jnp.log(sums)
    for m in range(tiles):
        first, second = total_log[:, 2 * m, :], total_log[:, 2 * m + 1, :]
        log_ref[:, m * LANES : (m + 1) * LANES] = jnp.where(low_line, first, swap_halves(second))

    def columns(a):
        share = jnp.exp(l_in[a] - total_log[...]).reshape(heads * 8, LANES)
        missing = LANES - heads * 8
        if missing:
            share = jnp.concatenate([share, jnp.zeros((missing, LANES), jnp.float32)], axis=0)
        return jnp.transpose(share)

    def add_group(a, carry):
        weight[a] = columns(a)
        return carry

    spread(add_group, 0)
    for ch in range(pairs):
        for m in range(tiles):

            def add_part(a, sums, ch=ch, m=m):
                t0 = o_in[a, 2 * ch, m].astype(jnp.float32)
                t1 = o_in[a, 2 * ch + 1, m].astype(jnp.float32)
                parts = (jnp.where(low, t0, swap_halves(t1)), jnp.where(low, swap_halves(t0), t1))
                made = []
                for e in range(2):
                    at = 2 * ch * 8 + 2 * m + e
                    share = jnp.where(low, weight[a, :BLK, at : at + 1], weight[a, :BLK, at + 8 : at + 9])
                    made.append(sums[e] + parts[e] * share)
                return tuple(made)

            zero = jnp.zeros((BLK, LANES), jnp.float32)
            made = spread(add_part, (zero, zero))
            for e in range(2):
                r = 2 * m + e
                attended[r * BLK : (r + 1) * BLK, ch * LANES : (ch + 1) * LANES] = made[e].astype(jnp.bfloat16)

    out_rows = rows // splits
    tile_width = min(512, wo.shape[1])
    chunks = wo.shape[1] // tile_width
    peers = [lax.rem(tp + d, splits) for d in range(splits)]

    def partial_of(d, c):
        mine = attended[pl.ds(pl.multiple_of(peers[d] * out_rows, out_rows), out_rows), :]
        made = jnp.dot(mine, wo[:, c * tile_width : (c + 1) * tile_width], preferred_element_type=jnp.float32)
        return made.astype(jnp.bfloat16)

    def hop(d, c):
        return pltpu.make_async_remote_copy(
            src_ref=stage.at[d - 1, c],
            dst_ref=landed_ref.at[d - 1, c],
            send_sem=tp_send.at[d - 1, c],
            recv_sem=tp_recv.at[d - 1, c],
            device_id={"tp": peers[d]},
            device_id_type=MESH,
        )

    for d in range(1, splits):
        for c in range(chunks):
            stage[d - 1, c] = partial_of(d, c)
            hop(d, c).start()
    for c in range(chunks):
        mine_ref[c] = partial_of(0, c)

    def sent(copy):
        copy.wait_send()

    for i in range(pairs):
        for e in range(2):
            head = 2 * pair_of(i) + e

            def drain(i=i, e=e, head=head):
                kv_copy(2 * i + e, head).wait_send()
                q_copy(2 * i + e, first_device + head).wait_send()

            if i < pairs - 1:
                drain()
            else:
                pl.when(head != idx)(drain)

    def drain_down(a, carry):
        for i in range(pairs):
            for e in range(2):
                q_copy(2 * i + e, a * heads + 2 * pair_of(i) + e).wait_send()
        return carry

    lax.fori_loop(0, group, drain_down, 0)

    def drain_results(t, carry):
        j = (group + lax.div(t, heads)) * heads + lax.rem(idx + t, heads)
        o_copy(j).wait_send()
        l_copy(j).wait_send()
        return carry

    lax.fori_loop(1, devices - first_device, drain_results, 0)
    for d in range(1, splits):
        for c in range(chunks):
            hop(d, c).wait()


def local(devices, splits, tokens, w_query, w_key, w_value, w_out, chosen):
    rows, depth = tokens.shape
    width = w_query.shape[1]
    out_width = w_out.shape[1]
    heads = width // HEAD_DIM
    pairs = heads // 2
    groups = devices // heads
    blocks = rows // BLK
    tiles = blocks // 2
    half = HEAD_DIM // 2
    wide = 2 if pairs % 2 == 0 else 1

    inverse = rotary_base ** (-np.arange(half, dtype=np.float64) / half)
    within = np.tile(np.arange(rows)[:, None] * inverse[None, :], (1, LANES // half))
    start = np.tile((np.arange(devices) * rows)[:, None] * inverse[None, :], (1, LANES // half))
    cos_table = jnp.asarray(np.cos(within), jnp.float32)
    sin_table = jnp.asarray(np.sin(within), jnp.float32)
    base = jnp.asarray(np.stack([np.cos(start), np.sin(start)]), jnp.float32)

    out_rows = rows // splits
    tile_width = min(512, out_width)
    chunks = out_width // tile_width
    dma = pltpu.SemaphoreType.DMA
    bf16, f32 = jnp.bfloat16, jnp.float32
    mine, landed, logs = pl.pallas_call(
        functools.partial(layer_kernel, devices, splits),
        in_specs=[in_smem()] + [in_hbm()] * 7 + [in_vmem()],
        out_specs=[in_vmem()] * 3,
        out_shape=[
            jax.ShapeDtypeStruct((chunks, out_rows, tile_width), bf16),
            jax.ShapeDtypeStruct((splits - 1, chunks, out_rows, tile_width), bf16),
            jax.ShapeDtypeStruct((heads, rows), f32),
        ],
        scratch_shapes=[
            pltpu.VMEM((rows, depth), bf16),
            pltpu.VMEM((pairs // wide, depth, wide * LANES), bf16),
            pltpu.VMEM((pairs, depth, 2 * LANES), bf16),
            pltpu.VMEM((width, out_width), bf16),
            pltpu.VMEM((rows, LANES), f32),
            pltpu.VMEM((rows, LANES), f32),
            pltpu.VMEM((heads, blocks, BLK, LANES), bf16),
            pltpu.VMEM((heads, tiles, BLK, LANES), bf16),
            pltpu.VMEM((heads, blocks, BLK, LANES), bf16),
            pltpu.VMEM((heads, blocks, BLK, LANES), bf16),
            pltpu.VMEM((devices, tiles, BLK, LANES), bf16),
            pltpu.VMEM((devices, tiles, BLK, LANES), bf16),
            pltpu.VMEM((devices, 8, LANES), f32),
            pltpu.VMEM((groups, heads, tiles, BLK, LANES), bf16),
            pltpu.VMEM((groups, heads, 8, LANES), f32),
            pltpu.VMEM((groups, LANES, LANES), f32),
            pltpu.VMEM((heads, 8, LANES), f32),
            pltpu.VMEM((rows, width), bf16),
            pltpu.VMEM((splits - 1, chunks, out_rows, tile_width), bf16),
            dma((7, pairs)),
            dma((heads,)),
            dma((heads,)),
            dma((devices,)),
            dma((devices,)),
            dma((devices,)),
            dma((devices,)),
            dma((devices,)),
            dma((devices,)),
            dma((splits - 1, chunks)),
            dma((splits - 1, chunks)),
        ],
        compiler_params=pltpu.CompilerParams(
            collective_id=0, has_side_effects=True, vmem_limit_bytes=VMEM_LIMIT
        ),
        name="layer",
    )(jnp.transpose(chosen), tokens, w_query, w_key, w_value, w_out, cos_table, sin_table, base)
    total = mine.astype(f32) + jnp.sum(landed.astype(f32), axis=0)
    mixed = jnp.transpose(total.astype(bf16), (1, 0, 2)).reshape(out_rows, out_width)
    return mixed, logs


def solution(mesh):
    placed = (P("kv", None), P(None, "tp"), P(None, "tp"), P(None, "tp"), P("tp", None), P())
    return jax.shard_map(
        functools.partial(local, mesh.shape["kv"], mesh.shape["tp"]),
        mesh=mesh,
        in_specs=placed,
        out_specs=(P(("kv", "tp"), None), P("tp", "kv")),
        check_vma=False,
    )
```

time: 66.8 us -> 59.6 us (0.89)
  the two profiles are of different devices: /device:TPU:25 before, /device:TPU:21 now
where the time goes in v1:
time: 59.6 us; the launch traced here: 59.3 us
  Pallas kernels  55.4 us (93%)
  local copies, waits for them, and re-layouts  1.89 us (3%)
  other arithmetic  1.34 us (2%)
  between operations  0.66 us (1%)
    pallas_call x1, Pallas kernels, local(): pl.pallas_call(functools.partial(layer_kernel, devices, splits), in_specs...  55.4 us
    unnamed x4, local copies, waits for them, and re-layouts  1.62 us
    transpose x1, other arithmetic, local(): jnp.transpose(total.astype(bf16), (1, 0, 2)).reshape(out_rows, out_width)  1.34 us

profile of v1, /device:TPU:21, one launch (start us, length us, event | category | flops | bytes accessed | tf_op | source)
XLA Modules:
  0.0 59.3 jit_solution(4017293583664474895)
XLA Ops:
  0.6 55.4 %layer.1 = (bf16[4,128,512]{2,1,0:T(8,128)(2,1)}, bf16[1,4,128,512]{3,2,1,0:T(8,128)(2,1)}, f32[8,256]{1,0:T(8,128)}) custom-call(s32[16,64]{1,0:T(8,128)} %bitcast.8, bf16[256,2048]{1,0:T(8,128)(2,1)} %x_ref.1, bf16[2048,512]{1,0:T(8,128)(2,1)} %wq_ref.1, bf16[2048,512]{1,0:T(8,128)(2,1)} %wk_ref.1, bf16[2048,512]{1,0:T(8,128)(2,1)} %wv_ref.1, ...), custom_call_target="tpu_custom_call" | custom-call | tf_op jit(solution)/shard_map/layer/pallas_call | solution.py:488
  56.0 0.0 copy-start
  56.1 1.3 %fusion.1 = bf16[128,4,512]{2,0,1:T(8,128)(2,1)S(1)} fusion(bf16[4,128,512]{2,1,0:T(8,128)(2,1)} %get-tuple-element.5, bf16[1,4,128,512]{3,2,1,0:T(8,128)(2,1)} %get-tuple-element.6), kind=kLoop, calls=%fused_computation.2 | loop fusion | flops 1048576 | bytes 1572864 | tf_op jit(solution)/shard_map/transpose | solution.py:535
  57.4 0.3 copy.11
  57.7 1.0 %copy.12 = bf16[128,2048]{1,0:T(8,128)(2,1)} copy(bf16[128,2048]{0,1:T(8,128)(2,1)S(1)} %bitcast.7) | data formatting | bytes 1048576
  58.7 0.0 copy-done
  58.7 0.6 %copy.14 = f32[8,256]{1,0:T(8,128)} copy(f32[8,256]{1,0:T(8,128)S(1)} %copy-done) | data formatting | bytes 16384
Async XLA Ops:
  56.0 2.6 %copy-start = (f32[8,256]{1,0:T(8,128)S(1)}, f32[8,256]{1,0:T(8,128)}, u32[]{:S(2)}) copy-start(f32[8,256]{1,0:T(8,128)} %get-tuple-element.13) | copy-start | bytes 24580

commit v2 on v1

--- a/solution.py
+++ b/solution.py
@@ -12,6 +12,7 @@
 BLK = 64
 LANES = 128
 VMEM_LIMIT = 65_000_000
+AHEAD = 2
 
 rotary_base = 500000.0
 masked_score = -1e30
@@ -21,10 +22,6 @@
 
 def in_vmem():
     return pl.BlockSpec(memory_space=pltpu.VMEM)
-
-
-def in_smem():
-    return pl.BlockSpec(memory_space=pltpu.SMEM)
 
 
 def in_hbm():
@@ -38,7 +35,7 @@
 def layer_kernel(
     devices, splits, chosen_ref, x_ref, wq_ref, wk_ref, wv_ref, wo_ref, cos_ref, sin_ref, base_ref,
     mine_ref, landed_ref, log_ref,
-    x, wq, wkv, wo, cos_t, sin_t, kv_out, q_out, kv_in, vk_in, q_in, o_out, l_out, o_in, l_in, weight, total_log,
+    x, wq, wkv, wo, cos_t, sin_t, kv_out, q_out, kv_in, vk_in, lists, place_v, place_s, bias, q_in, o_out, l_out, o_in, l_in, weight, total_log,
     attended, stage, load_sem, kv_send, kv_recv, q_send, q_recv, o_send, o_recv, l_send, l_recv, tp_send, tp_recv,
 ):
     heads = kv_out.shape[0]
@@ -79,7 +76,11 @@
     load_sin = pltpu.make_async_copy(sin_ref, sin_t, load_sem.at[5, 0])
     load_o = pltpu.make_async_copy(wo_ref, wo, load_sem.at[6, 0])
 
+    load_lists = pltpu.make_async_copy(chosen_ref, lists, load_sem.at[7, 0])
+    move_places = pltpu.make_async_copy(place_v, place_s, load_sem.at[8, 0])
+
     load_x.start()
+    load_lists.start()
     load_cos.start()
     load_sin.start()
     for i in range(pairs):
@@ -105,7 +106,7 @@
     def kv_copy(slot, head):
         return pltpu.make_async_remote_copy(
             src_ref=kv_out.at[slot],
-            dst_ref=kv_in.at[idx],
+            dst_ref=kv_in.at[pl.ds(idx * blocks, blocks)],
             send_sem=kv_send.at[head],
             recv_sem=kv_recv.at[idx],
             device_id={"kv": first_device + head},
@@ -222,9 +223,25 @@
 
     lax.fori_loop(0, group, send_down, 0)
 
+    load_lists.wait()
+    place = lists[...] - first_device * blocks
+    held = (place >= 0) & (place < table_blocks)
+    place_v[...] = jnp.where(held, place, 0)
+    move_places.start()
+    column = lax.broadcasted_iota(jnp.int32, (entries, entries * BLK), 1)
+    slot = column // (8 * BLK) * 8 + column // BLK % 4 * 2 + column // (4 * BLK) % 2
+    unit = (slot == lax.broadcasted_iota(jnp.int32, slot.shape, 0)).astype(jnp.float32)
+    bias[...] = masked_score * (
+        1.0
+        - lax.dot_general(
+            jnp.where(held, 1.0, 0.0), unit, (((0,), (0,)), ((), ())), preferred_element_type=jnp.float32
+        )
+    )
+    move_places.wait()
+
     own_slot = 2 * (pairs - 1) + lax.rem(idx, 2)
     for r in range(blocks):
-        kv_in[idx, r] = kv_out[own_slot, r]
+        kv_in[idx * blocks + r] = kv_out[own_slot, r]
     for m in range(tiles):
         q_in[me, m] = q_out[own_slot, m]
 
@@ -237,74 +254,67 @@
 
         @pl.when(k > 0)
         def _():
-            arrival(kv_in.at[source], kv_recv.at[source]).wait_recv()
+            arrival(kv_in.at[pl.ds(source * blocks, blocks)], kv_recv.at[source]).wait_recv()
 
         for r in range(blocks):
-            vk_in[source, r] = swap_halves(kv_in[source, r].astype(jnp.float32)).astype(jnp.bfloat16)
+            place = source * blocks + r
+            vk_in[place] = swap_halves(kv_in[place].astype(jnp.float32)).astype(jnp.bfloat16)
         return carry
 
     lax.fori_loop(0, heads, take_kv, 0)
 
     def attend(j):
-        logs = jnp.zeros((BLK, LANES), jnp.float32)
+        stacks = []
         for m in range(tiles):
             tile = q_in[j, m]
             swapped = swap_halves(tile.astype(jnp.float32)).astype(jnp.bfloat16)
             none = jnp.zeros_like(tile)
-            results = []
-            for e in range(2):
-                r = 2 * m + e
-                at_low, at_high = (tile, swapped) if e == 0 else (swapped, tile)
-                stacked = jnp.concatenate([jnp.where(low, at_low, none), jnp.where(low, none, at_high)], axis=0)
-                bias, places = [], []
-                for s in range(entries):
-                    place = chosen_ref[s, j * blocks + r] - first_device * blocks
-                    held = (place >= 0) & (place < table_blocks)
-                    bias.append(jnp.where(held, 0.0, masked_score).astype(jnp.float32))
-                    places.append(jnp.where(held, place, 0))
-                scores, values = [], []
-                for lower in range(0, entries, 8):
-                    keys_here, values_here = [], []
-                    for s in range(lower, lower + 8, 2):
-                        a_place, b_place = places[s], places[s + 1]
-                        a = kv_in[lax.div(a_place, blocks), lax.rem(a_place, blocks)]
-                        b = vk_in[lax.div(b_place, blocks), lax.rem(b_place, blocks)]
-                        keys_here.append(jnp.where(low, a, b))
-                        values_here.append(jnp.where(low, b, a))
-                    made = lax.dot_general(
-                        stacked, jnp.concatenate(keys_here, axis=0), (((1,), (1,)), ((), ())),
-                        preferred_element_type=jnp.float32,
-                    )
-                    lines = []
-                    for first in range(2):
-                        lines.append(
-                            jnp.concatenate(
-                                [
-                                    jnp.where(low_line, bias[s + first], bias[s + 2 + first])
-                                    for s in range(lower, lower + 8, 4)
-                                ],
-                                axis=1,
-                            )
-                        )
-                    scores.append((made[:BLK] + lines[0], made[BLK:] + lines[1]))
-                    values.append(jnp.concatenate(values_here, axis=0))
-                top = functools.reduce(jnp.maximum, [part for both in scores for part in both])
-                top = jnp.max(top, axis=1, keepdims=True)
-                total = 0.0
-                made = 0.0
-                for both, held_values in zip(scores, values):
-                    weights = [jnp.exp(part - top) for part in both]
-                    total = total + weights[0] + weights[1]
-                    rounded = jnp.concatenate([part.astype(jnp.bfloat16) for part in weights], axis=0)
-                    made = made + jnp.dot(rounded, held_values, preferred_element_type=jnp.float32)
-                total = jnp.sum(total, axis=1, keepdims=True)
-                if e == 0:
-                    summed = swap_halves(made[:BLK]) + made[BLK:]
-                else:
-                    summed = made[:BLK] + swap_halves(made[BLK:])
-                results.append(summed / total)
-                logs = jnp.where(lane == r, top + jnp.log(total), logs)
-            o_out[j, m] = jnp.where(low, results[0], results[1]).astype(jnp.bfloat16)
+            for at_low, at_high in ((tile, swapped), (swapped, tile)):
+                stacks.append(jnp.concatenate([jnp.where(low, at_low, none), jnp.where(low, none, at_high)], axis=0))
+
+        def score(r):
+            scores, values = [], []
+            for lower in range(0, entries, 8):
+                keys_here, values_here = [], []
+                for s in range(lower, lower + 8, 2):
+                    a = kv_in[place_s[s, j * blocks + r]]
+                    b = vk_in[place_s[s + 1, j * blocks + r]]
+                    keys_here.append(jnp.where(low, a, b))
+                    values_here.append(jnp.where(low, b, a))
+                made = lax.dot_general(
+                    stacks[r], jnp.concatenate(keys_here, axis=0), (((1,), (1,)), ((), ())),
+                    preferred_element_type=jnp.float32,
+                )
+                line = bias[pl.ds(j * blocks + r, 1), lower * BLK : (lower + 8) * BLK]
+                scores += [made[:BLK] + line[:, : 4 * BLK], made[BLK:] + line[:, 4 * BLK :]]
+                values.append(jnp.concatenate(values_here, axis=0))
+            top = jnp.max(functools.reduce(jnp.maximum, scores), axis=1, keepdims=True)
+            return scores, values, top
+
+        def gather(r, scores, values, top):
+            weights = [jnp.exp(part - top) for part in scores]
+            total = jnp.sum(functools.reduce(jnp.add, weights), axis=1, keepdims=True)
+            made = 0.0
+            for k, held_values in enumerate(values):
+                rounded = jnp.concatenate([part.astype(jnp.bfloat16) for part in weights[2 * k : 2 * k + 2]], axis=0)
+                made = made + jnp.dot(rounded, held_values, preferred_element_type=jnp.float32)
+            if r % 2 == 0:
+                summed = swap_halves(made[:BLK]) + made[BLK:]
+            else:
+                summed = made[:BLK] + swap_halves(made[BLK:])
+            return summed / total, top + jnp.log(total)
+
+        ready, results = [], []
+        for r in range(blocks + AHEAD):
+            if r < blocks:
+                ready.append(score(r))
+            if r >= AHEAD:
+                results.append(gather(r - AHEAD, *ready[r - AHEAD]))
+        logs = jnp.zeros((BLK, LANES), jnp.float32)
+        for r in range(blocks):
+            logs = jnp.where(lane == r, results[r][1], logs)
+        for m in range(tiles):
+            o_out[j, m] = jnp.where(low, results[2 * m][0], results[2 * m + 1][0]).astype(jnp.bfloat16)
         lines = jnp.transpose(jnp.concatenate([logs, jnp.zeros_like(logs)], axis=0))
         l_out[j] = lines[:8]
 
@@ -411,7 +421,7 @@
     def hop(d, c):
         return pltpu.make_async_remote_copy(
             src_ref=stage.at[d - 1, c],
-            dst_ref=landed_ref.at[d - 1, c],
+            dst_ref=landed_ref.at[d - 1, :, pl.ds(c * tile_width, tile_width)],
             send_sem=tp_send.at[d - 1, c],
             recv_sem=tp_recv.at[d - 1, c],
             device_id={"tp": peers[d]},
@@ -423,7 +433,7 @@
             stage[d - 1, c] = partial_of(d, c)
             hop(d, c).start()
     for c in range(chunks):
-        mine_ref[c] = partial_of(0, c)
+        mine_ref[:, c * tile_width : (c + 1) * tile_width] = partial_of(0, c)
 
     def sent(copy):
         copy.wait_send()
@@ -487,11 +497,11 @@
     bf16, f32 = jnp.bfloat16, jnp.float32
     mine, landed, logs = pl.pallas_call(
         functools.partial(layer_kernel, devices, splits),
-        in_specs=[in_smem()] + [in_hbm()] * 7 + [in_vmem()],
+        in_specs=[in_hbm()] * 8 + [in_vmem()],
         out_specs=[in_vmem()] * 3,
         out_shape=[
-            jax.ShapeDtypeStruct((chunks, out_rows, tile_width), bf16),
-            jax.ShapeDtypeStruct((splits - 1, chunks, out_rows, tile_width), bf16),
+            jax.ShapeDtypeStruct((out_rows, out_width), bf16),
+            jax.ShapeDtypeStruct((splits - 1, out_rows, out_width), bf16),
             jax.ShapeDtypeStruct((heads, rows), f32),
         ],
         scratch_shapes=[
@@ -503,8 +513,12 @@
             pltpu.VMEM((rows, LANES), f32),
             pltpu.VMEM((heads, blocks, BLK, LANES), bf16),
             pltpu.VMEM((heads, tiles, BLK, LANES), bf16),
-            pltpu.VMEM((heads, blocks, BLK, LANES), bf16),
-            pltpu.VMEM((heads, blocks, BLK, LANES), bf16),
+            pltpu.VMEM((heads * blocks, BLK, LANES), bf16),
+            pltpu.VMEM((heads * blocks, BLK, LANES), bf16),
+            pltpu.VMEM(chosen.shape[::-1], jnp.int32),
+            pltpu.VMEM(chosen.shape[::-1], jnp.int32),
+            pltpu.SMEM(chosen.shape[::-1], jnp.int32),
+            pltpu.VMEM((chosen.shape[0], chosen.shape[1] * BLK), f32),
             pltpu.VMEM((devices, tiles, BLK, LANES), bf16),
             pltpu.VMEM((devices, tiles, BLK, LANES), bf16),
             pltpu.VMEM((devices, 8, LANES), f32),
@@ -514,7 +528,7 @@
             pltpu.VMEM((heads, 8, LANES), f32),
             pltpu.VMEM((rows, width), bf16),
             pltpu.VMEM((splits - 1, chunks, out_rows, tile_width), bf16),
-            dma((7, pairs)),
+            dma((9, pairs)),
             dma((heads,)),
             dma((heads,)),
             dma((devices,)),
@@ -532,8 +546,7 @@
         name="layer",
     )(jnp.transpose(chosen), tokens, w_query, w_key, w_value, w_out, cos_table, sin_table, base)
     total = mine.astype(f32) + jnp.sum(landed.astype(f32), axis=0)
-    mixed = jnp.transpose(total.astype(bf16), (1, 0, 2)).reshape(out_rows, out_width)
-    return mixed, logs
+    return total.astype(bf16), logs
 
 
 def solution(mesh):

time: 59.6 us -> 51.7 us (0.87)
  the two profiles are of different devices: /device:TPU:21 before, /device:TPU:25 now
where the time goes in v2:
time: 51.7 us; the launch traced here: 51.4 us
  Pallas kernels  47.3 us (91%)
  other arithmetic  2.12 us (4%)
  local copies, waits for them, and re-layouts  1.29 us (2%)
  between operations  0.64 us (1%)
    pallas_call x1, Pallas kernels, local(): pl.pallas_call(functools.partial(layer_kernel, devices, splits), in_specs...  47.3 us
    convert_element_type x1, other arithmetic, local(): return (total.astype(bf16), logs)  2.12 us
    unnamed x1, local copies, waits for them, and re-layouts  1.29 us

profile of v2, /device:TPU:25, one launch (start us, length us, event | category | flops | bytes accessed | tf_op | source)
XLA Modules:
  0.0 51.4 jit_solution(9103035646481837581)
XLA Ops:
  0.6 47.3 %layer.1 = (bf16[128,2048]{1,0:T(8,128)(2,1)}, bf16[1,128,2048]{2,1,0:T(8,128)(2,1)}, f32[8,256]{1,0:T(8,128)}) custom-call(s32[16,64]{1,0:T(8,128)} %bitcast.4, bf16[256,2048]{1,0:T(8,128)(2,1)} %x_ref.1, bf16[2048,512]{1,0:T(8,128)(2,1)} %wq_ref.1, bf16[2048,512]{1,0:T(8,128)(2,1)} %wk_ref.1, bf16[2048,512]{1,0:T(8,128)(2,1)} %wv_ref.1, ...), custom_call_target="tpu_custom_call" | custom-call | tf_op jit(solution)/shard_map/layer/pallas_call | solution.py:498
  48.0 2.1 %fusion = bf16[128,2048]{1,0:T(8,128)(2,1)} fusion(bf16[128,2048]{1,0:T(8,128)(2,1)} %get-tuple-element.5, bf16[1,128,2048]{2,1,0:T(8,128)(2,1)} %get-tuple-element.6), kind=kLoop, calls=%fused_computation.1 | loop fusion | flops 1048576 | bytes 1572864 | tf_op jit(solution)/shard_map/convert_element_type | solution.py:549
  50.1 1.3 %copy.12 = f32[8,256]{1,0:T(8,128)} copy(f32[8,256]{1,0:T(8,128)} %get-tuple-element.11) | data formatting | bytes 16384

commit v3 on v2

--- a/solution.py
+++ b/solution.py
@@ -11,7 +11,7 @@
 HEAD_DIM = 64
 BLK = 64
 LANES = 128
-VMEM_LIMIT = 65_000_000
+VMEM_LIMIT = 55_000_000
 AHEAD = 2
 
 rotary_base = 500000.0
@@ -33,9 +33,9 @@
 
 
 def layer_kernel(
-    devices, splits, chosen_ref, x_ref, wq_ref, wk_ref, wv_ref, wo_ref, cos_ref, sin_ref, base_ref,
+    devices, splits, chosen_ref, x_ref, wq_ref, wk_ref, wv_ref, wo_ref,
     mine_ref, landed_ref, log_ref,
-    x, wq, wkv, wo, cos_t, sin_t, kv_out, q_out, kv_in, vk_in, lists, place_v, place_s, bias, q_in, o_out, l_out, o_in, l_in, weight, total_log,
+    x, wq, wkv, wo, kv_out, q_out, kv_in, vk_in, place_v, place_s, bias, q_in, o_out, l_out, o_in, l_in, weight, total_log,
     attended, stage, load_sem, kv_send, kv_recv, q_send, q_recv, o_send, o_recv, l_send, l_recv, tp_send, tp_recv,
 ):
     heads = kv_out.shape[0]
@@ -56,7 +56,7 @@
     half = HEAD_DIM // 2
 
     def pair_of(i):
-        return lax.rem(lax.div(idx, 2) + 1 + i, pairs)
+        return lax.rem(lax.div(idx, 2) + pairs - i, pairs)
 
     def strip(ref, i):
         return ref.at[:, pl.ds(pl.multiple_of(pair_of(i) * LANES, LANES), LANES)]
@@ -72,23 +72,16 @@
         return pltpu.make_async_copy(strip(wv_ref, i), wkv.at[i, :, pl.ds(LANES, LANES)], load_sem.at[2, i])
 
     load_x = pltpu.make_async_copy(x_ref, x, load_sem.at[3, 0])
-    load_cos = pltpu.make_async_copy(cos_ref, cos_t, load_sem.at[4, 0])
-    load_sin = pltpu.make_async_copy(sin_ref, sin_t, load_sem.at[5, 0])
-    load_o = pltpu.make_async_copy(wo_ref, wo, load_sem.at[6, 0])
-
-    load_lists = pltpu.make_async_copy(chosen_ref, lists, load_sem.at[7, 0])
-    move_places = pltpu.make_async_copy(place_v, place_s, load_sem.at[8, 0])
+    load_o = pltpu.make_async_copy(wo_ref, wo, load_sem.at[4, 0])
+
+    move_places = pltpu.make_async_copy(place_v, place_s, load_sem.at[6, 0])
 
     load_x.start()
-    load_lists.start()
-    load_cos.start()
-    load_sin.start()
     for i in range(pairs):
         load_k(i).start()
         load_v(i).start()
-        if i % wide == 0:
-            for e in range(wide):
-                load_q(i + e).start()
+    for i in range(pairs):
+        load_q(i).start()
     load_o.start()
 
     barrier = pltpu.get_barrier_semaphore()
@@ -150,14 +143,24 @@
         )
 
     load_x.wait()
-    load_cos.wait()
-    load_sin.wait()
     low_rows = lax.broadcasted_iota(jnp.int32, (rows, LANES), 1) < LANES // 2
     turn_low = lax.broadcasted_iota(jnp.int32, (rows, LANES), 1) % HEAD_DIM < half
-    cos_base = base_ref[0, pl.ds(me, 1), :]
-    sin_base = base_ref[1, pl.ds(me, 1), :]
-    cos_part = cos_t[...] * cos_base - sin_t[...] * sin_base
-    sin_part = sin_t[...] * cos_base + cos_t[...] * sin_base
+
+    def angles(count, step, start):
+        channel = (lax.broadcasted_iota(jnp.int32, (count, LANES), 1) % half).astype(jnp.float32)
+        position = lax.broadcasted_iota(jnp.int32, (count, LANES), 0) * step + start
+        turn = position.astype(jnp.float32) * jnp.exp(channel * (-np.log(rotary_base) / half))
+        return jnp.cos(turn), jnp.sin(turn)
+
+    cos_fine, sin_fine = angles(8, 1, 0)
+    cos_coarse, sin_coarse = angles(rows // 8, 8, me * rows)
+    cos_parts, sin_parts = [], []
+    for k in range(rows // 8):
+        cos_k, sin_k = cos_coarse[k : k + 1], sin_coarse[k : k + 1]
+        cos_parts.append(cos_k * cos_fine - sin_k * sin_fine)
+        sin_parts.append(sin_k * cos_fine + cos_k * sin_fine)
+    cos_part = jnp.concatenate(cos_parts, axis=0)
+    sin_part = jnp.concatenate(sin_parts, axis=0)
     sin_part = jnp.where(turn_low, -sin_part, sin_part)
 
     def turned(part):
@@ -193,7 +196,7 @@
     def send_kv(i):
         for e in range(2):
             head = 2 * pair_of(i) + e
-            if i < pairs - 1:
+            if i > 0:
                 kv_copy(2 * i + e, head).start()
             else:
                 pl.when(head != idx)(lambda e=e, head=head: kv_copy(2 * i + e, head).start())
@@ -201,7 +204,7 @@
     def send_q(i):
         for e in range(2):
             head = 2 * pair_of(i) + e
-            if i < pairs - 1:
+            if i > 0:
                 q_copy(2 * i + e, first_device + head).start()
             else:
                 pl.when(head != idx)(lambda e=e, head=head: q_copy(2 * i + e, first_device + head).start())
@@ -211,9 +214,10 @@
         if i == 0:
             pl.semaphore_wait(barrier, devices - 1 + splits - 1)
         send_kv(i)
-        if i % wide == 0:
-            make_q(i)
-        send_q(i)
+    for i in range(0, pairs, wide):
+        make_q(i)
+        for e in range(wide):
+            send_q(i + e)
 
     def send_down(a, carry):
         for i in range(pairs):
@@ -223,8 +227,7 @@
 
     lax.fori_loop(0, group, send_down, 0)
 
-    load_lists.wait()
-    place = lists[...] - first_device * blocks
+    place = chosen_ref[...] - first_device * blocks
     held = (place >= 0) & (place < table_blocks)
     place_v[...] = jnp.where(held, place, 0)
     move_places.start()
@@ -239,7 +242,7 @@
     )
     move_places.wait()
 
-    own_slot = 2 * (pairs - 1) + lax.rem(idx, 2)
+    own_slot = lax.rem(idx, 2)
     for r in range(blocks):
         kv_in[idx * blocks + r] = kv_out[own_slot, r]
     for m in range(tiles):
@@ -318,9 +321,19 @@
         lines = jnp.transpose(jnp.concatenate([logs, jnp.zeros_like(logs)], axis=0))
         l_out[j] = lines[:8]
 
+    def served(t):
+        opening = heads // 2
+        cycle = 2 * (groups - group) - 1
+        after = jnp.maximum(t - opening, 0)
+        owns = lax.div(after, cycle)
+        own = (t < opening) | (lax.rem(after, cycle) == cycle - 1)
+        visitor = after - owns
+        step = jnp.where(own, jnp.where(t < opening, t, opening + owns), visitor)
+        target = group + jnp.where(own, 0, 1 + lax.div(visitor, heads))
+        return target * heads + lax.rem(idx + lax.rem(step, heads), heads)
+
     def serve(t, carry):
-        other_group = group + lax.div(t, heads)
-        j = other_group * heads + lax.rem(idx + t, heads)
+        j = served(t)
 
         @pl.when(t > 0)
         def _():
@@ -446,7 +459,7 @@
                 kv_copy(2 * i + e, head).wait_send()
                 q_copy(2 * i + e, first_device + head).wait_send()
 
-            if i < pairs - 1:
+            if i > 0:
                 drain()
             else:
                 pl.when(head != idx)(drain)
@@ -460,7 +473,7 @@
     lax.fori_loop(0, group, drain_down, 0)
 
     def drain_results(t, carry):
-        j = (group + lax.div(t, heads)) * heads + lax.rem(idx + t, heads)
+        j = served(t)
         o_copy(j).wait_send()
         l_copy(j).wait_send()
         return carry
@@ -480,15 +493,7 @@
     groups = devices // heads
     blocks = rows // BLK
     tiles = blocks // 2
-    half = HEAD_DIM // 2
     wide = 2 if pairs % 2 == 0 else 1
-
-    inverse = rotary_base ** (-np.arange(half, dtype=np.float64) / half)
-    within = np.tile(np.arange(rows)[:, None] * inverse[None, :], (1, LANES // half))
-    start = np.tile((np.arange(devices) * rows)[:, None] * inverse[None, :], (1, LANES // half))
-    cos_table = jnp.asarray(np.cos(within), jnp.float32)
-    sin_table = jnp.asarray(np.sin(within), jnp.float32)
-    base = jnp.asarray(np.stack([np.cos(start), np.sin(start)]), jnp.float32)
 
     out_rows = rows // splits
     tile_width = min(512, out_width)
@@ -497,7 +502,7 @@
     bf16, f32 = jnp.bfloat16, jnp.float32
     mine, landed, logs = pl.pallas_call(
         functools.partial(layer_kernel, devices, splits),
-        in_specs=[in_hbm()] * 8 + [in_vmem()],
+        in_specs=[in_vmem()] + [in_hbm()] * 5,
         out_specs=[in_vmem()] * 3,
         out_shape=[
             jax.ShapeDtypeStruct((out_rows, out_width), bf16),
@@ -509,13 +514,10 @@
             pltpu.VMEM((pairs // wide, depth, wide * LANES), bf16),
             pltpu.VMEM((pairs, depth, 2 * LANES), bf16),
             pltpu.VMEM((width, out_width), bf16),
-            pltpu.VMEM((rows, LANES), f32),
-            pltpu.VMEM((rows, LANES), f32),
             pltpu.VMEM((heads, blocks, BLK, LANES), bf16),
             pltpu.VMEM((heads, tiles, BLK, LANES), bf16),
             pltpu.VMEM((heads * blocks, BLK, LANES), bf16),
             pltpu.VMEM((heads * blocks, BLK, LANES), bf16),
-            pltpu.VMEM(chosen.shape[::-1], jnp.int32),
             pltpu.VMEM(chosen.shape[::-1], jnp.int32),
             pltpu.SMEM(chosen.shape[::-1], jnp.int32),
             pltpu.VMEM((chosen.shape[0], chosen.shape[1] * BLK), f32),
@@ -528,7 +530,7 @@
             pltpu.VMEM((heads, 8, LANES), f32),
             pltpu.VMEM((rows, width), bf16),
             pltpu.VMEM((splits - 1, chunks, out_rows, tile_width), bf16),
-            dma((9, pairs)),
+            dma((7, pairs)),
             dma((heads,)),
             dma((heads,)),
             dma((devices,)),
@@ -544,7 +546,7 @@
             collective_id=0, has_side_effects=True, vmem_limit_bytes=VMEM_LIMIT
         ),
         name="layer",
-    )(jnp.transpose(chosen), tokens, w_query, w_key, w_value, w_out, cos_table, sin_table, base)
+    )(jnp.transpose(chosen), tokens, w_query, w_key, w_value, w_out)
     total = mine.astype(f32) + jnp.sum(landed.astype(f32), axis=0)
     return total.astype(bf16), logs
 

time: 51.7 us -> 45.6 us (0.88)
  the two profiles are of different devices: /device:TPU:25 before, /device:TPU:0 now
where the time goes in v3:
time: 45.6 us; the launch traced here: 45.4 us
  Pallas kernels  42.5 us (93%)
  local copies, waits for them, and re-layouts  1.29 us (3%)
  other arithmetic  0.92 us (2%)
  between operations  0.65 us (1%)
    pallas_call x1, Pallas kernels, local(): pl.pallas_call(functools.partial(layer_kernel, devices, splits), in_specs...  42.5 us
    unnamed x3, local copies, waits for them, and re-layouts  1.29 us
    convert_element_type x1, other arithmetic, local(): return (total.astype(bf16), logs)  0.92 us

profile of v3, /device:TPU:0, one launch (start us, length us, event | category | flops | bytes accessed | tf_op | source)
XLA Modules:
  0.0 45.4 jit_solution(15605601872001287620)
XLA Ops:
  0.6 0.0 copy-start
  0.6 0.7 %copy-done = s32[64,16]{0,1:T(8,128)S(1)} copy-done((s32[64,16]{0,1:T(8,128)S(1)}, s32[64,16]{0,1:T(8,128)}, u32[]{:S(2)}) %copy-start) | copy-done | bytes 4120
  1.3 42.5 %layer.1 = (bf16[128,2048]{1,0:T(8,128)(2,1)S(1)}, bf16[1,128,2048]{2,1,0:T(8,128)(2,1)S(1)}, f32[8,256]{1,0:T(8,128)S(1)}) custom-call(s32[16,64]{1,0:T(8,128)S(1)} %bitcast.4, bf16[256,2048]{1,0:T(8,128)(2,1)} %x_ref.1, bf16[2048,512]{1,0:T(8,128)(2,1)} %wq_ref.1, bf16[2048,512]{1,0:T(8,128)(2,1)} %wk_ref.1, bf16[2048,512]{1,0:T(8,128)(2,1)} %wv_ref.1, ...), custom_call_target="tpu_custom_call" | custom-call | tf_op jit(solution)/shard_map/layer/pallas_call | solution.py:503
  43.9 0.9 %fusion = bf16[128,2048]{1,0:T(8,128)(2,1)} fusion(bf16[128,2048]{1,0:T(8,128)(2,1)S(1)} %get-tuple-element.5, bf16[1,128,2048]{2,1,0:T(8,128)(2,1)S(1)} %get-tuple-element.6), kind=kLoop, calls=%fused_computation.1 | loop fusion | flops 1048576 | bytes 1572864 | tf_op jit(solution)/shard_map/convert_element_type | solution.py:551
  44.8 0.6 %copy.9 = f32[8,256]{1,0:T(8,128)} copy(f32[8,256]{1,0:T(8,128)S(1)} %get-tuple-element.11) | data formatting | bytes 16384
Async XLA Ops:
  0.6 0.7 %copy-start = (s32[64,16]{0,1:T(8,128)S(1)}, s32[64,16]{0,1:T(8,128)}, u32[]{:S(2)}) copy-start(s32[64,16]{0,1:T(8,128)} %param.11) | copy-start | bytes 12292

commit v4 on v3

--- a/solution.py
+++ b/solution.py
@@ -13,6 +13,7 @@
 LANES = 128
 VMEM_LIMIT = 55_000_000
 AHEAD = 2
+LOG2_E = float(np.log2(np.e))
 
 rotary_base = 500000.0
 masked_score = -1e30
@@ -35,8 +36,8 @@
 def layer_kernel(
     devices, splits, chosen_ref, x_ref, wq_ref, wk_ref, wv_ref, wo_ref,
     mine_ref, landed_ref, log_ref,
-    x, wq, wkv, wo, kv_out, q_out, kv_in, vk_in, place_v, place_s, bias, q_in, o_out, l_out, o_in, l_in, weight, total_log,
-    attended, stage, load_sem, kv_send, kv_recv, q_send, q_recv, o_send, o_recv, l_send, l_recv, tp_send, tp_recv,
+    x, wq, wkv, wo, kv_out, q_out, kv_in, vk_in, place_v, place_s, bias, q_in, o_out, l_out, o_in, l_in, total_log,
+    attended, stage, load_sem, kv_load, q_load, kv_send, kv_recv, q_send, q_recv, o_send, o_recv, l_send, l_recv, tp_send, tp_recv,
 ):
     heads = kv_out.shape[0]
     pairs = heads // 2
@@ -63,18 +64,20 @@
 
     def load_q(i):
         target = wq.at[i // wide, :, pl.ds((i % wide) * LANES, LANES)]
-        return pltpu.make_async_copy(strip(wq_ref, i), target, load_sem.at[0, i])
+        return pltpu.make_async_copy(strip(wq_ref, i), target, q_load.at[i // wide])
 
     def load_k(i):
-        return pltpu.make_async_copy(strip(wk_ref, i), wkv.at[i, :, pl.ds(0, LANES)], load_sem.at[1, i])
+        return pltpu.make_async_copy(strip(wk_ref, i), wkv.at[i, :, pl.ds(0, LANES)], kv_load.at[i])
 
     def load_v(i):
-        return pltpu.make_async_copy(strip(wv_ref, i), wkv.at[i, :, pl.ds(LANES, LANES)], load_sem.at[2, i])
-
-    load_x = pltpu.make_async_copy(x_ref, x, load_sem.at[3, 0])
-    load_o = pltpu.make_async_copy(wo_ref, wo, load_sem.at[4, 0])
-
-    move_places = pltpu.make_async_copy(place_v, place_s, load_sem.at[6, 0])
+        return pltpu.make_async_copy(strip(wv_ref, i), wkv.at[i, :, pl.ds(LANES, LANES)], kv_load.at[i])
+
+    def loaded(ref, semaphore):
+        pltpu.make_async_copy(ref, ref, semaphore).wait()
+
+    load_x = pltpu.make_async_copy(x_ref, x, load_sem.at[0])
+    load_o = pltpu.make_async_copy(wo_ref, wo, load_sem.at[1])
+    move_places = pltpu.make_async_copy(place_v, place_s, load_sem.at[2])
 
     load_x.start()
     for i in range(pairs):
@@ -100,8 +103,8 @@
         return pltpu.make_async_remote_copy(
             src_ref=kv_out.at[slot],
             dst_ref=kv_in.at[pl.ds(idx * blocks, blocks)],
-            send_sem=kv_send.at[head],
-            recv_sem=kv_recv.at[idx],
+            send_sem=kv_send.at[0],
+            recv_sem=kv_recv.at[0],
             device_id={"kv": first_device + head},
             device_id_type=MESH,
         )
@@ -110,7 +113,7 @@
         return pltpu.make_async_remote_copy(
             src_ref=q_out.at[slot],
             dst_ref=q_in.at[me],
-            send_sem=q_send.at[target],
+            send_sem=q_send.at[lax.div(target, heads)],
             recv_sem=q_recv.at[me],
             device_id={"kv": target},
             device_id_type=MESH,
@@ -120,8 +123,8 @@
         return pltpu.make_async_remote_copy(
             src_ref=o_out.at[target],
             dst_ref=o_in.at[group, idx],
-            send_sem=o_send.at[target],
-            recv_sem=o_recv.at[me],
+            send_sem=o_send.at[lax.div(target, heads)],
+            recv_sem=o_recv.at[group, lax.div(idx, 2)],
             device_id={"kv": target},
             device_id_type=MESH,
         )
@@ -130,15 +133,15 @@
         return pltpu.make_async_remote_copy(
             src_ref=l_out.at[target],
             dst_ref=l_in.at[group, idx],
-            send_sem=l_send.at[target],
-            recv_sem=l_recv.at[me],
+            send_sem=l_send.at[lax.div(target, heads)],
+            recv_sem=l_recv.at[group, lax.div(idx, 2)],
             device_id={"kv": target},
             device_id_type=MESH,
         )
 
-    def arrival(copy, semaphore):
+    def arrival(ref, semaphore):
         return pltpu.make_async_remote_copy(
-            src_ref=copy, dst_ref=copy, send_sem=semaphore, recv_sem=semaphore,
+            src_ref=ref, dst_ref=ref, send_sem=semaphore, recv_sem=semaphore,
             device_id={"kv": me}, device_id_type=MESH,
         )
 
@@ -168,8 +171,7 @@
         return part * cos_part + other * sin_part
 
     def make_kv(i):
-        load_k(i).wait()
-        load_v(i).wait()
+        loaded(wkv.at[i], kv_load.at[i])
         made = jnp.dot(x[...], wkv[i], preferred_element_type=jnp.float32)
         keys = turned(made[:, :LANES])
         values = made[:, LANES:]
@@ -180,11 +182,10 @@
             kv_out[2 * i + 1, r] = odd[r * BLK : (r + 1) * BLK]
 
     def make_q(i):
-        for e in range(wide):
-            load_q(i + e).wait()
+        loaded(wq.at[i // wide], q_load.at[i // wide])
         made = jnp.dot(x[...], wq[i // wide], preferred_element_type=jnp.float32)
         for e in range(wide):
-            part = turned(made[:, e * LANES : (e + 1) * LANES]) * (HEAD_DIM**-0.5)
+            part = turned(made[:, e * LANES : (e + 1) * LANES]) * (HEAD_DIM**-0.5 * LOG2_E)
             swapped = swap_halves(part)
             low = low_rows[:BLK]
             for m in range(tiles):
@@ -216,16 +217,15 @@
         send_kv(i)
     for i in range(0, pairs, wide):
         make_q(i)
-        for e in range(wide):
-            send_q(i + e)
+        if i == 0:
+            for e in range(wide):
+                send_q(e)
 
     def send_down(a, carry):
         for i in range(pairs):
             for e in range(2):
                 q_copy(2 * i + e, a * heads + 2 * pair_of(i) + e).start()
         return carry
-
-    lax.fori_loop(0, group, send_down, 0)
 
     place = chosen_ref[...] - first_device * blocks
     held = (place >= 0) & (place < table_blocks)
@@ -252,74 +252,79 @@
     lane = lax.broadcasted_iota(jnp.int32, (BLK, LANES), 1)
     low_line = lax.broadcasted_iota(jnp.int32, (1, LANES), 1) < LANES // 2
 
-    def take_kv(k, carry):
-        source = lax.rem(idx + k, heads)
-
-        @pl.when(k > 0)
-        def _():
-            arrival(kv_in.at[pl.ds(source * blocks, blocks)], kv_recv.at[source]).wait_recv()
-
+    arrival(kv_in.at[pl.ds(0, (heads - 1) * blocks)], kv_recv.at[0]).wait_recv()
+    for i in range(wide, pairs):
+        send_q(i)
+    lax.fori_loop(0, group, send_down, 0)
+
+    def swap_kv(k, carry):
         for r in range(blocks):
-            place = source * blocks + r
+            place = k * blocks + r
             vk_in[place] = swap_halves(kv_in[place].astype(jnp.float32)).astype(jnp.bfloat16)
         return carry
 
-    lax.fori_loop(0, heads, take_kv, 0)
-
-    def attend(j):
+    lax.fori_loop(0, heads, swap_kv, 0)
+
+    def attend(js):
         stacks = []
-        for m in range(tiles):
-            tile = q_in[j, m]
-            swapped = swap_halves(tile.astype(jnp.float32)).astype(jnp.bfloat16)
-            none = jnp.zeros_like(tile)
-            for at_low, at_high in ((tile, swapped), (swapped, tile)):
-                stacks.append(jnp.concatenate([jnp.where(low, at_low, none), jnp.where(low, none, at_high)], axis=0))
-
-        def score(r):
+        for j in js:
+            for m in range(tiles):
+                tile = q_in[j, m]
+                swapped = swap_halves(tile.astype(jnp.float32)).astype(jnp.bfloat16)
+                none = jnp.zeros_like(tile)
+                for at_low, at_high in ((tile, swapped), (swapped, tile)):
+                    stacks.append(
+                        jnp.concatenate([jnp.where(low, at_low, none), jnp.where(low, none, at_high)], axis=0)
+                    )
+
+        def score(n):
+            block = js[n // blocks] * blocks + n % blocks
             scores, values = [], []
             for lower in range(0, entries, 8):
                 keys_here, values_here = [], []
                 for s in range(lower, lower + 8, 2):
-                    a = kv_in[place_s[s, j * blocks + r]]
-                    b = vk_in[place_s[s + 1, j * blocks + r]]
+                    a = kv_in[place_s[s, block]]
+                    b = vk_in[place_s[s + 1, block]]
                     keys_here.append(jnp.where(low, a, b))
                     values_here.append(jnp.where(low, b, a))
                 made = lax.dot_general(
-                    stacks[r], jnp.concatenate(keys_here, axis=0), (((1,), (1,)), ((), ())),
+                    stacks[n], jnp.concatenate(keys_here, axis=0), (((1,), (1,)), ((), ())),
                     preferred_element_type=jnp.float32,
                 )
-                line = bias[pl.ds(j * blocks + r, 1), lower * BLK : (lower + 8) * BLK]
+                line = bias[pl.ds(block, 1), lower * BLK : (lower + 8) * BLK]
                 scores += [made[:BLK] + line[:, : 4 * BLK], made[BLK:] + line[:, 4 * BLK :]]
                 values.append(jnp.concatenate(values_here, axis=0))
             top = jnp.max(functools.reduce(jnp.maximum, scores), axis=1, keepdims=True)
             return scores, values, top
 
-        def gather(r, scores, values, top):
-            weights = [jnp.exp(part - top) for part in scores]
+        def gather(n, scores, values, top):
+            weights = [jnp.exp2(part - top) for part in scores]
             total = jnp.sum(functools.reduce(jnp.add, weights), axis=1, keepdims=True)
             made = 0.0
             for k, held_values in enumerate(values):
                 rounded = jnp.concatenate([part.astype(jnp.bfloat16) for part in weights[2 * k : 2 * k + 2]], axis=0)
                 made = made + jnp.dot(rounded, held_values, preferred_element_type=jnp.float32)
-            if r % 2 == 0:
+            if n % 2 == 0:
                 summed = swap_halves(made[:BLK]) + made[BLK:]
             else:
                 summed = made[:BLK] + swap_halves(made[BLK:])
-            return summed / total, top + jnp.log(total)
+            return summed / total, (top + jnp.log2(total)) * (1.0 / LOG2_E)
 
         ready, results = [], []
-        for r in range(blocks + AHEAD):
-            if r < blocks:
-                ready.append(score(r))
-            if r >= AHEAD:
-                results.append(gather(r - AHEAD, *ready[r - AHEAD]))
-        logs = jnp.zeros((BLK, LANES), jnp.float32)
-        for r in range(blocks):
-            logs = jnp.where(lane == r, results[r][1], logs)
-        for m in range(tiles):
-            o_out[j, m] = jnp.where(low, results[2 * m][0], results[2 * m + 1][0]).astype(jnp.bfloat16)
-        lines = jnp.transpose(jnp.concatenate([logs, jnp.zeros_like(logs)], axis=0))
-        l_out[j] = lines[:8]
+        for n in range(len(js) * blocks + AHEAD):
+            if n < len(js) * blocks:
+                ready.append(score(n))
+            if n >= AHEAD:
+                results.append(gather(n - AHEAD, *ready[n - AHEAD]))
+        for k, j in enumerate(js):
+            found = results[k * blocks : (k + 1) * blocks]
+            logs = jnp.zeros((BLK, LANES), jnp.float32)
+            for r in range(blocks):
+                logs = jnp.where(lane == r, found[r][1], logs)
+            for m in range(tiles):
+                o_out[j, m] = jnp.where(low, found[2 * m][0], found[2 * m + 1][0]).astype(jnp.bfloat16)
+            lines = jnp.transpose(jnp.concatenate([logs, jnp.zeros_like(logs)], axis=0))
+            l_out[j] = lines[:8]
 
     def served(t):
         opening = heads // 2
@@ -332,29 +337,33 @@
         target = group + jnp.where(own, 0, 1 + lax.div(visitor, heads))
         return target * heads + lax.rem(idx + lax.rem(step, heads), heads)
 
-    def serve(t, carry):
-        j = served(t)
-
-        @pl.when(t > 0)
+    def serve(u, carry):
+        js = [served(2 * u), served(2 * u + 1)]
+
+        @pl.when(u > 0)
         def _():
-            arrival(q_in.at[j], q_recv.at[j]).wait_recv()
-
-        attend(j)
-
-        @pl.when(t > 0)
+            arrival(q_in.at[js[0]], q_recv.at[js[0]]).wait_recv()
+
+        arrival(q_in.at[js[1]], q_recv.at[js[1]]).wait_recv()
+        attend(js)
+
+        @pl.when(u > 0)
         def _():
-            o_copy(j).start()
-            l_copy(j).start()
-
-        @pl.when(t == 0)
+            o_copy(js[0]).start()
+            l_copy(js[0]).start()
+
+        o_copy(js[1]).start()
+        l_copy(js[1]).start()
+
+        @pl.when(u == 0)
         def _():
             for m in range(tiles):
-                o_in[group, idx, m] = o_out[j, m]
-            l_in[group, idx] = l_out[j]
-
-        return carry
-
-    lax.fori_loop(0, devices - first_device, serve, 0)
+                o_in[group, idx, m] = o_out[js[0], m]
+            l_in[group, idx] = l_out[js[0]]
+
+        return carry
+
+    lax.fori_loop(0, (devices - first_device) // 2, serve, 0)
 
     def absent(a, carry):
         o_in[a] = jnp.zeros(o_in.shape[1:], o_in.dtype)
@@ -362,18 +371,6 @@
         return carry
 
     lax.fori_loop(group + 1, groups, absent, 0)
-
-    def take_results(k, carry):
-        source = lax.rem(me + k, (group + 1) * heads)
-        place = o_in.at[lax.div(source, heads), lax.rem(source, heads)]
-        arrival(place, o_recv.at[source]).wait_recv()
-        line = l_in.at[lax.div(source, heads), lax.rem(source, heads)]
-        arrival(line, l_recv.at[source]).wait_recv()
-        return carry
-
-    lax.fori_loop(1, (group + 1) * heads, take_results, 0)
-
-    load_o.wait()
 
     def spread(body, start):
         if groups <= 2:
@@ -382,45 +379,58 @@
             return start
         return lax.fori_loop(0, groups, body, start)
 
-    highest = spread(lambda a, top: jnp.maximum(top, l_in[a]), jnp.full(l_in.shape[1:], masked_score, jnp.float32))
-    sums = spread(lambda a, acc: acc + jnp.exp(l_in[a] - highest), jnp.zeros(l_in.shape[1:], jnp.float32))
-    total_log[...] = highest + jnp.log(sums)
+    for i in range(pairs):
+        ch = pair_of(i)
+
+        def take_results(a, carry, i=i, ch=ch):
+            def take(count):
+                o_place = o_in.at[a, pl.ds(2 * ch, count)]
+                arrival(o_place, o_recv.at[a, ch]).wait_recv()
+                l_place = l_in.at[a, pl.ds(2 * ch, count)]
+                arrival(l_place, l_recv.at[a, ch]).wait_recv()
+
+            if i > 0:
+                take(2)
+            else:
+                pl.when(a == group)(lambda: take(1))
+                pl.when(a != group)(lambda: take(2))
+            return carry
+
+        lax.fori_loop(0, group + 1, take_results, 0)
+
+        def lines(a, ch=ch):
+            return l_in[a, pl.ds(2 * ch, 2)]
+
+        start = jnp.full((2, 8, LANES), masked_score, jnp.float32)
+        highest = spread(lambda a, top: jnp.maximum(top, lines(a)), start)
+        sums = spread(lambda a, acc: acc + jnp.exp(lines(a) - highest), jnp.zeros_like(start))
+        logs = highest + jnp.log(sums)
+        total_log[pl.ds(2 * ch, 2)] = logs
+
+        def add_share(a, parts, ch=ch, logs=logs):
+            share = jnp.exp(lines(a) - logs).reshape(16, LANES)
+            columns = jnp.transpose(jnp.concatenate([share, jnp.zeros((LANES - 16, LANES), jnp.float32)], axis=0))
+            made = []
+            for m in range(tiles):
+                t0 = o_in[a, 2 * ch, m].astype(jnp.float32)
+                t1 = o_in[a, 2 * ch + 1, m].astype(jnp.float32)
+                both = (jnp.where(low, t0, swap_halves(t1)), jnp.where(low, swap_halves(t0), t1))
+                for e in range(2):
+                    r = 2 * m + e
+                    scale = jnp.where(low, columns[:BLK, r : r + 1], columns[:BLK, 8 + r : 9 + r])
+                    made.append(parts[r] + both[e] * scale)
+            return tuple(made)
+
+        made = spread(add_share, tuple(jnp.zeros((BLK, LANES), jnp.float32) for _ in range(blocks)))
+        for r in range(blocks):
+            columns = pl.ds(pl.multiple_of(ch * LANES, LANES), LANES)
+            attended[r * BLK : (r + 1) * BLK, columns] = made[r].astype(jnp.bfloat16)
+
     for m in range(tiles):
         first, second = total_log[:, 2 * m, :], total_log[:, 2 * m + 1, :]
         log_ref[:, m * LANES : (m + 1) * LANES] = jnp.where(low_line, first, swap_halves(second))
 
-    def columns(a):
-        share = jnp.exp(l_in[a] - total_log[...]).reshape(heads * 8, LANES)
-        missing = LANES - heads * 8
-        if missing:
-            share = jnp.concatenate([share, jnp.zeros((missing, LANES), jnp.float32)], axis=0)
-        return jnp.transpose(share)
-
-    def add_group(a, carry):
-        weight[a] = columns(a)
-        return carry
-
-    spread(add_group, 0)
-    for ch in range(pairs):
-        for m in range(tiles):
-
-            def add_part(a, sums, ch=ch, m=m):
-                t0 = o_in[a, 2 * ch, m].astype(jnp.float32)
-                t1 = o_in[a, 2 * ch + 1, m].astype(jnp.float32)
-                parts = (jnp.where(low, t0, swap_halves(t1)), jnp.where(low, swap_halves(t0), t1))
-                made = []
-                for e in range(2):
-                    at = 2 * ch * 8 + 2 * m + e
-                    share = jnp.where(low, weight[a, :BLK, at : at + 1], weight[a, :BLK, at + 8 : at + 9])
-                    made.append(sums[e] + parts[e] * share)
-                return tuple(made)
-
-            zero = jnp.zeros((BLK, LANES), jnp.float32)
-            made = spread(add_part, (zero, zero))
-            for e in range(2):
-                r = 2 * m + e
-                attended[r * BLK : (r + 1) * BLK, ch * LANES : (ch + 1) * LANES] = made[e].astype(jnp.bfloat16)
-
+    load_o.wait()
     out_rows = rows // splits
     tile_width = min(512, wo.shape[1])
     chunks = wo.shape[1] // tile_width
@@ -435,8 +445,8 @@
         return pltpu.make_async_remote_copy(
             src_ref=stage.at[d - 1, c],
             dst_ref=landed_ref.at[d - 1, :, pl.ds(c * tile_width, tile_width)],
-            send_sem=tp_send.at[d - 1, c],
-            recv_sem=tp_recv.at[d - 1, c],
+            send_sem=tp_send.at[d - 1],
+            recv_sem=tp_recv.at[d - 1],
             device_id={"tp": peers[d]},
             device_id_type=MESH,
         )
@@ -448,40 +458,29 @@
     for c in range(chunks):
         mine_ref[:, c * tile_width : (c + 1) * tile_width] = partial_of(0, c)
 
-    def sent(copy):
-        copy.wait_send()
-
-    for i in range(pairs):
-        for e in range(2):
-            head = 2 * pair_of(i) + e
-
-            def drain(i=i, e=e, head=head):
-                kv_copy(2 * i + e, head).wait_send()
-                q_copy(2 * i + e, first_device + head).wait_send()
-
-            if i > 0:
-                drain()
-            else:
-                pl.when(head != idx)(drain)
-
-    def drain_down(a, carry):
-        for i in range(pairs):
-            for e in range(2):
-                q_copy(2 * i + e, a * heads + 2 * pair_of(i) + e).wait_send()
-        return carry
-
-    lax.fori_loop(0, group, drain_down, 0)
-
-    def drain_results(t, carry):
-        j = served(t)
-        o_copy(j).wait_send()
-        l_copy(j).wait_send()
-        return carry
-
-    lax.fori_loop(1, devices - first_device, drain_results, 0)
+    def sent(ref, semaphore):
+        arrival(ref, semaphore).wait_send()
+
+    sent(kv_out.at[pl.ds(0, heads - 1)], kv_send.at[0])
+    sent(q_out.at[pl.ds(0, heads - 1)], q_send.at[group])
+
+    def sent_down(a, carry):
+        sent(q_out, q_send.at[a])
+        return carry
+
+    lax.fori_loop(0, group, sent_down, 0)
+    sent(o_out.at[pl.ds(0, heads - 1)], o_send.at[group])
+    sent(l_out.at[pl.ds(0, heads - 1)], l_send.at[group])
+
+    def sent_up(a, carry):
+        sent(o_out.at[pl.ds(0, heads)], o_send.at[a])
+        sent(l_out.at[pl.ds(0, heads)], l_send.at[a])
+        return carry
+
+    lax.fori_loop(group + 1, groups, sent_up, 0)
     for d in range(1, splits):
-        for c in range(chunks):
-            hop(d, c).wait()
+        sent(stage.at[d - 1], tp_send.at[d - 1])
+        arrival(landed_ref.at[d - 1], tp_recv.at[d - 1]).wait_recv()
 
 
 def local(devices, splits, tokens, w_query, w_key, w_value, w_out, chosen):
@@ -526,21 +525,22 @@
             pltpu.VMEM((devices, 8, LANES), f32),
             pltpu.VMEM((groups, heads, tiles, BLK, LANES), bf16),
             pltpu.VMEM((groups, heads, 8, LANES), f32),
-            pltpu.VMEM((groups, LANES, LANES), f32),
             pltpu.VMEM((heads, 8, LANES), f32),
             pltpu.VMEM((rows, width), bf16),
             pltpu.VMEM((splits - 1, chunks, out_rows, tile_width), bf16),
-            dma((7, pairs)),
-            dma((heads,)),
-            dma((heads,)),
+            dma((3,)),
+            dma((pairs,)),
+            dma((pairs // wide,)),
+            dma((1,)),
+            dma((1,)),
+            dma((groups,)),
             dma((devices,)),
-            dma((devices,)),
-            dma((devices,)),
-            dma((devices,)),
-            dma((devices,)),
-            dma((devices,)),
-            dma((splits - 1, chunks)),
-            dma((splits - 1, chunks)),
+            dma((groups,)),
+            dma((groups, pairs)),
+            dma((groups,)),
+            dma((groups, pairs)),
+            dma((splits - 1,)),
+            dma((splits - 1,)),
         ],
         compiler_params=pltpu.CompilerParams(
             collective_id=0, has_side_effects=True, vmem_limit_bytes=VMEM_LIMIT

time: 45.6 us -> 47.3 us (1.037)
  Pallas kernels: 42.5 us -> 44.2 us
    pallas_call x1, Pallas kernels: 42.5 us -> 44.2 us  [local(): pl.pallas_call(functools.partial(layer_kernel, devices, splits), in_specs...]
where the time goes in v4:
time: 47.3 us; the launch traced here: 47.1 us
  Pallas kernels  44.2 us (93%)
  local copies, waits for them, and re-layouts  1.29 us (3%)
  other arithmetic  0.92 us (2%)
  between operations  0.65 us (1%)
    pallas_call x1, Pallas kernels, local(): pl.pallas_call(functools.partial(layer_kernel, devices, splits), in_specs...  44.2 us
    unnamed x3, local copies, waits for them, and re-layouts  1.29 us

profile of v4, /device:TPU:0, one launch (start us, length us, event | category | flops | bytes accessed | tf_op | source)
XLA Modules:
  0.0 47.1 jit_solution(5499060429465598110)
XLA Ops:
  0.6 0.0 copy-start
  0.6 0.7 %copy-done = s32[64,16]{0,1:T(8,128)S(1)} copy-done((s32[64,16]{0,1:T(8,128)S(1)}, s32[64,16]{0,1:T(8,128)}, u32[]{:S(2)}) %copy-start) | copy-done | bytes 4120
  1.3 44.2 %layer.1 = (bf16[128,2048]{1,0:T(8,128)(2,1)S(1)}, bf16[1,128,2048]{2,1,0:T(8,128)(2,1)S(1)}, f32[8,256]{1,0:T(8,128)S(1)}) custom-call(s32[16,64]{1,0:T(8,128)S(1)} %bitcast.4, bf16[256,2048]{1,0:T(8,128)(2,1)} %x_ref.1, bf16[2048,512]{1,0:T(8,128)(2,1)} %wq_ref.1, bf16[2048,512]{1,0:T(8,128)(2,1)} %wk_ref.1, bf16[2048,512]{1,0:T(8,128)(2,1)} %wv_ref.1, ...), custom_call_target="tpu_custom_call" | custom-call | tf_op jit(solution)/shard_map/layer/pallas_call | solution.py:502
  45.6 0.9 %fusion = bf16[128,2048]{1,0:T(8,128)(2,1)} fusion(bf16[128,2048]{1,0:T(8,128)(2,1)S(1)} %get-tuple-element.5, bf16[1,128,2048]{2,1,0:T(8,128)(2,1)S(1)} %get-tuple-element.6), kind=kLoop, calls=%fused_computation.1 | loop fusion | flops 1048576 | bytes 1572864 | tf_op jit(solution)/shard_map/convert_element_type | solution.py:551
  46.5 0.6 %copy.9 = f32[8,256]{1,0:T(8,128)} copy(f32[8,256]{1,0:T(8,128)S(1)} %get-tuple-element.11) | data formatting | bytes 16384
Async XLA Ops:
  0.6 0.7 %copy-start = (s32[64,16]{0,1:T(8,128)S(1)}, s32[64,16]{0,1:T(8,128)}, u32[]{:S(2)}) copy-start(s32[64,16]{0,1:T(8,128)} %param.11) | copy-start | bytes 12292

commit v5 on v4

--- a/solution.py
+++ b/solution.py
@@ -27,6 +27,16 @@
 
 def in_hbm():
     return pl.BlockSpec(memory_space=pltpu.HBM)
+
+
+def partner(place, step, count):
+    if count & (count - 1):
+        return lax.rem(place + step, count)
+    mixed, bit = 0, 1
+    while bit < count:
+        mixed = mixed + bit * lax.rem(lax.div(place, bit) + lax.div(step, bit), 2)
+        bit *= 2
+    return mixed
 
 
 def swap_halves(tile):
@@ -57,7 +67,7 @@
     half = HEAD_DIM // 2
 
     def pair_of(i):
-        return lax.rem(lax.div(idx, 2) + pairs - i, pairs)
+        return partner(lax.div(idx, 2), jnp.int32(i), pairs)
 
     def strip(ref, i):
         return ref.at[:, pl.ds(pl.multiple_of(pair_of(i) * LANES, LANES), LANES)]
@@ -80,12 +90,20 @@
     move_places = pltpu.make_async_copy(place_v, place_s, load_sem.at[2])
 
     load_x.start()
-    for i in range(pairs):
-        load_k(i).start()
-        load_v(i).start()
-    for i in range(pairs):
-        load_q(i).start()
-    load_o.start()
+    lowest = group == 0
+    early = min(2, pairs)
+
+    def start_kv(first, last):
+        for i in range(first, last):
+            load_k(i).start()
+            load_v(i).start()
+
+    def start_q():
+        for i in range(pairs):
+            load_q(i).start()
+
+    pl.when(lowest)(lambda: start_kv(0, early))
+    pl.when(jnp.logical_not(lowest))(start_q)
 
     barrier = pltpu.get_barrier_semaphore()
 
@@ -146,6 +164,16 @@
         )
 
     load_x.wait()
+
+    @pl.when(lowest)
+    def _():
+        start_kv(early, pairs)
+        start_q()
+
+    @pl.when(jnp.logical_not(lowest))
+    def _():
+        start_kv(0, pairs)
+
     low_rows = lax.broadcasted_iota(jnp.int32, (rows, LANES), 1) < LANES // 2
     turn_low = lax.broadcasted_iota(jnp.int32, (rows, LANES), 1) % HEAD_DIM < half
 
@@ -210,22 +238,39 @@
             else:
                 pl.when(head != idx)(lambda e=e, head=head: q_copy(2 * i + e, first_device + head).start())
 
+    def send_down(near):
+        def send(a, carry):
+            for i in range(pairs):
+                ch = pair_of(i)
+
+                @pl.when((2 * ch >= heads // 2) == near)
+                def _(i=i, ch=ch):
+                    for e in range(2):
+                        q_copy(2 * i + e, a * heads + 2 * ch + e).start()
+
+            return carry
+
+        lax.fori_loop(0, group, send, 0)
+
+    def make_queries():
+        for i in range(0, pairs, wide):
+            make_q(i)
+
+    @pl.when(jnp.logical_not(lowest))
+    def _():
+        make_queries()
+        pl.semaphore_wait(barrier, devices - 1 + splits - 1)
+        send_down(True)
+
     for i in range(pairs):
         make_kv(i)
         if i == 0:
-            pl.semaphore_wait(barrier, devices - 1 + splits - 1)
+            pl.when(lowest)(lambda: pl.semaphore_wait(barrier, devices - 1 + splits - 1))
         send_kv(i)
-    for i in range(0, pairs, wide):
-        make_q(i)
-        if i == 0:
-            for e in range(wide):
-                send_q(e)
-
-    def send_down(a, carry):
-        for i in range(pairs):
-            for e in range(2):
-                q_copy(2 * i + e, a * heads + 2 * pair_of(i) + e).start()
-        return carry
+    pl.when(lowest)(make_queries)
+    for i in range(pairs):
+        send_q(i)
+    load_o.start()
 
     place = chosen_ref[...] - first_device * blocks
     held = (place >= 0) & (place < table_blocks)
@@ -253,9 +298,7 @@
     low_line = lax.broadcasted_iota(jnp.int32, (1, LANES), 1) < LANES // 2
 
     arrival(kv_in.at[pl.ds(0, (heads - 1) * blocks)], kv_recv.at[0]).wait_recv()
-    for i in range(wide, pairs):
-        send_q(i)
-    lax.fori_loop(0, group, send_down, 0)
+    send_down(False)
 
     def swap_kv(k, carry):
         for r in range(blocks):
@@ -324,42 +367,43 @@
             for m in range(tiles):
                 o_out[j, m] = jnp.where(low, found[2 * m][0], found[2 * m + 1][0]).astype(jnp.bfloat16)
             lines = jnp.transpose(jnp.concatenate([logs, jnp.zeros_like(logs)], axis=0))
-            l_out[j] = lines[:8]
+            for m in range(tiles):
+                first, second = lines[2 * m : 2 * m + 1], lines[2 * m + 1 : 2 * m + 2]
+                l_out[j, m : m + 1] = jnp.where(low_line, first, swap_halves(second))
+
+    visits = (groups - 1 - group) * heads
+    opening = jnp.where((idx < heads // 2) | (visits == 0), heads, 2)
 
     def served(t):
-        opening = heads // 2
-        cycle = 2 * (groups - group) - 1
-        after = jnp.maximum(t - opening, 0)
-        owns = lax.div(after, cycle)
-        own = (t < opening) | (lax.rem(after, cycle) == cycle - 1)
-        visitor = after - owns
-        step = jnp.where(own, jnp.where(t < opening, t, opening + owns), visitor)
-        target = group + jnp.where(own, 0, 1 + lax.div(visitor, heads))
-        return target * heads + lax.rem(idx + lax.rem(step, heads), heads)
+        visiting = (t >= opening) & (t < opening + visits)
+        visitor = jnp.where(visiting, t - opening, 0)
+        visitor = jnp.where(opening < heads, visitor, visits - 1 - visitor)
+        own = jnp.where(t < opening, t, jnp.where(visiting, 0, heads + 1 - (t - visits)))
+        target = group + jnp.where(visiting, 1 + lax.div(visitor, heads), 0)
+        step = jnp.where(visiting, lax.rem(visitor, heads), own)
+        return target * heads + partner(idx, step, heads)
 
     def serve(u, carry):
         js = [served(2 * u), served(2 * u + 1)]
-
-        @pl.when(u > 0)
-        def _():
-            arrival(q_in.at[js[0]], q_recv.at[js[0]]).wait_recv()
-
-        arrival(q_in.at[js[1]], q_recv.at[js[1]]).wait_recv()
+        for j in js:
+
+            @pl.when(j != me)
+            def _(j=j):
+                arrival(q_in.at[j], q_recv.at[j]).wait_recv()
+
         attend(js)
-
-        @pl.when(u > 0)
-        def _():
-            o_copy(js[0]).start()
-            l_copy(js[0]).start()
-
-        o_copy(js[1]).start()
-        l_copy(js[1]).start()
-
-        @pl.when(u == 0)
-        def _():
-            for m in range(tiles):
-                o_in[group, idx, m] = o_out[js[0], m]
-            l_in[group, idx] = l_out[js[0]]
+        for j in js:
+
+            @pl.when(j != me)
+            def _(j=j):
+                o_copy(j).start()
+                l_copy(j).start()
+
+            @pl.when(j == me)
+            def _(j=j):
+                for m in range(tiles):
+                    o_in[group, idx, m] = o_out[j, m]
+                l_in[group, idx] = l_out[j]
 
         return carry
 
@@ -401,15 +445,17 @@
         def lines(a, ch=ch):
             return l_in[a, pl.ds(2 * ch, 2)]
 
-        start = jnp.full((2, 8, LANES), masked_score, jnp.float32)
+        start = jnp.full((2, tiles, LANES), masked_score, jnp.float32)
         highest = spread(lambda a, top: jnp.maximum(top, lines(a)), start)
         sums = spread(lambda a, acc: acc + jnp.exp(lines(a) - highest), jnp.zeros_like(start))
         logs = highest + jnp.log(sums)
         total_log[pl.ds(2 * ch, 2)] = logs
 
         def add_share(a, parts, ch=ch, logs=logs):
-            share = jnp.exp(lines(a) - logs).reshape(16, LANES)
-            columns = jnp.transpose(jnp.concatenate([share, jnp.zeros((LANES - 16, LANES), jnp.float32)], axis=0))
+            share = jnp.exp(lines(a) - logs)
+            share = [share[e, m : m + 1] for e in range(2) for m in range(tiles)]
+            share.append(jnp.zeros((LANES - 2 * tiles, LANES), jnp.float32))
+            columns = jnp.transpose(jnp.concatenate(share, axis=0))
             made = []
             for m in range(tiles):
                 t0 = o_in[a, 2 * ch, m].astype(jnp.float32)
@@ -417,7 +463,8 @@
                 both = (jnp.where(low, t0, swap_halves(t1)), jnp.where(low, swap_halves(t0), t1))
                 for e in range(2):
                     r = 2 * m + e
-                    scale = jnp.where(low, columns[:BLK, r : r + 1], columns[:BLK, 8 + r : 9 + r])
+                    here = columns[e * BLK : (e + 1) * BLK]
+                    scale = jnp.where(low, here[:, m : m + 1], here[:, tiles + m : tiles + m + 1])
                     made.append(parts[r] + both[e] * scale)
             return tuple(made)
 
@@ -427,8 +474,7 @@
             attended[r * BLK : (r + 1) * BLK, columns] = made[r].astype(jnp.bfloat16)
 
     for m in range(tiles):
-        first, second = total_log[:, 2 * m, :], total_log[:, 2 * m + 1, :]
-        log_ref[:, m * LANES : (m + 1) * LANES] = jnp.where(low_line, first, swap_halves(second))
+        log_ref[:, m * LANES : (m + 1) * LANES] = total_log[:, m, :]
 
     load_o.wait()
     out_rows = rows // splits
@@ -436,14 +482,12 @@
     chunks = wo.shape[1] // tile_width
     peers = [lax.rem(tp + d, splits) for d in range(splits)]
 
-    def partial_of(d, c):
-        mine = attended[pl.ds(pl.multiple_of(peers[d] * out_rows, out_rows), out_rows), :]
-        made = jnp.dot(mine, wo[:, c * tile_width : (c + 1) * tile_width], preferred_element_type=jnp.float32)
-        return made.astype(jnp.bfloat16)
+    def own_rows(d):
+        return pl.ds(pl.multiple_of(peers[d] * out_rows, out_rows), out_rows)
 
     def hop(d, c):
         return pltpu.make_async_remote_copy(
-            src_ref=stage.at[d - 1, c],
+            src_ref=stage.at[c, own_rows(d)],
             dst_ref=landed_ref.at[d - 1, :, pl.ds(c * tile_width, tile_width)],
             send_sem=tp_send.at[d - 1],
             recv_sem=tp_recv.at[d - 1],
@@ -451,12 +495,22 @@
             device_id_type=MESH,
         )
 
-    for d in range(1, splits):
-        for c in range(chunks):
-            stage[d - 1, c] = partial_of(d, c)
+    def product(place, c):
+        columns = slice(c * tile_width, (c + 1) * tile_width)
+        made = jnp.dot(attended[place], wo[:, columns], preferred_element_type=jnp.float32)
+        stage[c, place] = made.astype(jnp.bfloat16)
+
+    for c in range(chunks):
+        if c < chunks - 1:
+            product(pl.ds(0, rows), c)
+        else:
+            for d in range(1, splits):
+                product(own_rows(d), c)
+        for d in range(1, splits):
             hop(d, c).start()
+    product(own_rows(0), chunks - 1)
     for c in range(chunks):
-        mine_ref[:, c * tile_width : (c + 1) * tile_width] = partial_of(0, c)
+        mine_ref[:, c * tile_width : (c + 1) * tile_width] = stage[c, own_rows(0)]
 
     def sent(ref, semaphore):
         arrival(ref, semaphore).wait_send()
@@ -479,7 +533,7 @@
 
     lax.fori_loop(group + 1, groups, sent_up, 0)
     for d in range(1, splits):
-        sent(stage.at[d - 1], tp_send.at[d - 1])
+        sent(stage.at[:, own_rows(d)], tp_send.at[d - 1])
         arrival(landed_ref.at[d - 1], tp_recv.at[d - 1]).wait_recv()
 
 
@@ -522,12 +576,12 @@
             pltpu.VMEM((chosen.shape[0], chosen.shape[1] * BLK), f32),
             pltpu.VMEM((devices, tiles, BLK, LANES), bf16),
             pltpu.VMEM((devices, tiles, BLK, LANES), bf16),
-            pltpu.VMEM((devices, 8, LANES), f32),
+            pltpu.VMEM((devices, tiles, LANES), f32),
             pltpu.VMEM((groups, heads, tiles, BLK, LANES), bf16),
-            pltpu.VMEM((groups, heads, 8, LANES), f32),
-            pltpu.VMEM((heads, 8, LANES), f32),
+            pltpu.VMEM((groups, heads, tiles, LANES), f32),
+            pltpu.VMEM((heads, tiles, LANES), f32),
             pltpu.VMEM((rows, width), bf16),
-            pltpu.VMEM((splits - 1, chunks, out_rows, tile_width), bf16),
+            pltpu.VMEM((chunks, rows, tile_width), bf16),
             dma((3,)),
             dma((pairs,)),
             dma((pairs // wide,)),

time: 47.3 us -> 41.1 us (0.87)
  the two profiles are of different devices: /device:TPU:0 before, /device:TPU:9 now
where the time goes in v5:
time: 41.1 us; the launch traced here: 40.9 us
  Pallas kernels  38 us (92%)
  local copies, waits for them, and re-layouts  1.29 us (3%)
  other arithmetic  0.92 us (2%)
  between operations  0.65 us (2%)
    pallas_call x1, Pallas kernels, local(): pl.pallas_call(functools.partial(layer_kernel, devices, splits), in_specs...  38 us
    unnamed x3, local copies, waits for them, and re-layouts  1.29 us
    convert_element_type x1, other arithmetic, local(): return (total.astype(bf16), logs)  0.92 us

profile of v5, /device:TPU:9, one launch (start us, length us, event | category | flops | bytes accessed | tf_op | source)
XLA Modules:
  0.0 40.9 jit_solution(11316993856345057352)
XLA Ops:
  0.6 0.0 copy-start
  0.6 0.7 %copy-done = s32[64,16]{0,1:T(8,128)S(1)} copy-done((s32[64,16]{0,1:T(8,128)S(1)}, s32[64,16]{0,1:T(8,128)}, u32[]{:S(2)}) %copy-start) | copy-done | bytes 4120
  1.3 38.0 %layer.1 = (bf16[128,2048]{1,0:T(8,128)(2,1)S(1)}, bf16[1,128,2048]{2,1,0:T(8,128)(2,1)S(1)}, f32[8,256]{1,0:T(8,128)S(1)}) custom-call(s32[16,64]{1,0:T(8,128)S(1)} %bitcast.4, bf16[256,2048]{1,0:T(8,128)(2,1)} %x_ref.1, bf16[2048,512]{1,0:T(8,128)(2,1)} %wq_ref.1, bf16[2048,512]{1,0:T(8,128)(2,1)} %wk_ref.1, bf16[2048,512]{1,0:T(8,128)(2,1)} %wv_ref.1, ...), custom_call_target="tpu_custom_call" | custom-call | tf_op jit(solution)/shard_map/layer/pallas_call | solution.py:556
  39.3 0.9 %fusion = bf16[128,2048]{1,0:T(8,128)(2,1)} fusion(bf16[128,2048]{1,0:T(8,128)(2,1)S(1)} %get-tuple-element.5, bf16[1,128,2048]{2,1,0:T(8,128)(2,1)S(1)} %get-tuple-element.6), kind=kLoop, calls=%fused_computation.1 | loop fusion | flops 1048576 | bytes 1572864 | tf_op jit(solution)/shard_map/convert_element_type | solution.py:605
  40.3 0.6 %copy.9 = f32[8,256]{1,0:T(8,128)} copy(f32[8,256]{1,0:T(8,128)S(1)} %get-tuple-element.11) | data formatting | bytes 16384
Async XLA Ops:
  0.6 0.7 %copy-start = (s32[64,16]{0,1:T(8,128)S(1)}, s32[64,16]{0,1:T(8,128)}, u32[]{:S(2)}) copy-start(s32[64,16]{0,1:T(8,128)} %param.11) | copy-start | bytes 12292

commit v6 on v5

--- a/solution.py
+++ b/solution.py
@@ -46,7 +46,7 @@
 def layer_kernel(
     devices, splits, chosen_ref, x_ref, wq_ref, wk_ref, wv_ref, wo_ref,
     mine_ref, landed_ref, log_ref,
-    x, wq, wkv, wo, kv_out, q_out, kv_in, vk_in, place_v, place_s, bias, q_in, o_out, l_out, o_in, l_in, total_log,
+    x, wq, wkv, wo, kv_out, q_out, kv_in, vk_in, lists, place_v, place_s, bias, q_in, o_out, l_out, o_in, l_in, total_log,
     attended, stage, load_sem, kv_load, q_load, kv_send, kv_recv, q_send, q_recv, o_send, o_recv, l_send, l_recv, tp_send, tp_recv,
 ):
     heads = kv_out.shape[0]
@@ -56,7 +56,7 @@
     tiles = blocks // 2
     rows = blocks * BLK
     entries = chosen_ref.shape[0]
-    table_blocks = heads * blocks
+    high = heads // 2
     wide = wq.shape[2] // LANES
 
     me = lax.axis_index("kv")
@@ -64,6 +64,7 @@
     group = lax.div(me, heads)
     idx = lax.rem(me, heads)
     first_device = group * heads
+    visited = idx >= high
     half = HEAD_DIM // 2
 
     def pair_of(i):
@@ -87,11 +88,13 @@
 
     load_x = pltpu.make_async_copy(x_ref, x, load_sem.at[0])
     load_o = pltpu.make_async_copy(wo_ref, wo, load_sem.at[1])
+    load_lists = pltpu.make_async_copy(chosen_ref, lists, load_sem.at[3])
     move_places = pltpu.make_async_copy(place_v, place_s, load_sem.at[2])
 
     load_x.start()
+    load_lists.start()
     lowest = group == 0
-    early = min(2, pairs)
+    early = 1
 
     def start_kv(first, last):
         for i in range(first, last):
@@ -117,13 +120,13 @@
     for d in range(1, splits):
         pl.semaphore_signal(barrier, inc=1, device_id={"tp": lax.rem(tp + d, splits)}, device_id_type=MESH)
 
-    def kv_copy(slot, head):
+    def kv_copy(slot, target):
         return pltpu.make_async_remote_copy(
             src_ref=kv_out.at[slot],
-            dst_ref=kv_in.at[pl.ds(idx * blocks, blocks)],
-            send_sem=kv_send.at[0],
-            recv_sem=kv_recv.at[0],
-            device_id={"kv": first_device + head},
+            dst_ref=kv_in.at[pl.ds(me * blocks, blocks)],
+            send_sem=kv_send.at[lax.div(target, heads)],
+            recv_sem=kv_recv.at[group],
+            device_id={"kv": target},
             device_id_type=MESH,
         )
 
@@ -226,9 +229,9 @@
         for e in range(2):
             head = 2 * pair_of(i) + e
             if i > 0:
-                kv_copy(2 * i + e, head).start()
+                kv_copy(2 * i + e, first_device + head).start()
             else:
-                pl.when(head != idx)(lambda e=e, head=head: kv_copy(2 * i + e, head).start())
+                pl.when(head != idx)(lambda e=e, head=head: kv_copy(2 * i + e, first_device + head).start())
 
     def send_q(i):
         for e in range(2):
@@ -238,19 +241,33 @@
             else:
                 pl.when(head != idx)(lambda e=e, head=head: q_copy(2 * i + e, first_device + head).start())
 
-    def send_down(near):
+    def send_down():
         def send(a, carry):
             for i in range(pairs):
-                ch = pair_of(i)
-
-                @pl.when((2 * ch >= heads // 2) == near)
-                def _(i=i, ch=ch):
-                    for e in range(2):
-                        q_copy(2 * i + e, a * heads + 2 * ch + e).start()
+                for e in range(2):
+                    head = 2 * pair_of(i) + e
+
+                    @pl.when(head >= high)
+                    def _(i=i, e=e, head=head):
+                        q_copy(2 * i + e, a * heads + head).start()
 
             return carry
 
         lax.fori_loop(0, group, send, 0)
+
+    def send_up():
+        def send(a, carry):
+            for i in range(pairs):
+                for e in range(2):
+                    head = 2 * pair_of(i) + e
+
+                    @pl.when(head < high)
+                    def _(i=i, e=e, head=head):
+                        kv_copy(2 * i + e, a * heads + head).start()
+
+            return carry
+
+        lax.fori_loop(group + 1, groups, send, 0)
 
     def make_queries():
         for i in range(0, pairs, wide):
@@ -260,21 +277,24 @@
     def _():
         make_queries()
         pl.semaphore_wait(barrier, devices - 1 + splits - 1)
-        send_down(True)
+        send_down()
 
     for i in range(pairs):
         make_kv(i)
         if i == 0:
             pl.when(lowest)(lambda: pl.semaphore_wait(barrier, devices - 1 + splits - 1))
         send_kv(i)
+    send_up()
     pl.when(lowest)(make_queries)
     for i in range(pairs):
         send_q(i)
     load_o.start()
 
-    place = chosen_ref[...] - first_device * blocks
-    held = (place >= 0) & (place < table_blocks)
-    place_v[...] = jnp.where(held, place, 0)
+    load_lists.wait()
+    place = lists[...]
+    lowest_block = jnp.where(visited, first_device * blocks, 0)
+    held = (place >= lowest_block) & (place < (first_device + heads) * blocks)
+    place_v[...] = jnp.where(held, place, lowest_block)
     move_places.start()
     column = lax.broadcasted_iota(jnp.int32, (entries, entries * BLK), 1)
     slot = column // (8 * BLK) * 8 + column // BLK % 4 * 2 + column // (4 * BLK) % 2
@@ -289,7 +309,7 @@
 
     own_slot = lax.rem(idx, 2)
     for r in range(blocks):
-        kv_in[idx * blocks + r] = kv_out[own_slot, r]
+        kv_in[me * blocks + r] = kv_out[own_slot, r]
     for m in range(tiles):
         q_in[me, m] = q_out[own_slot, m]
 
@@ -297,8 +317,7 @@
     lane = lax.broadcasted_iota(jnp.int32, (BLK, LANES), 1)
     low_line = lax.broadcasted_iota(jnp.int32, (1, LANES), 1) < LANES // 2
 
-    arrival(kv_in.at[pl.ds(0, (heads - 1) * blocks)], kv_recv.at[0]).wait_recv()
-    send_down(False)
+    arrival(kv_in.at[pl.ds(0, (heads - 1) * blocks)], kv_recv.at[group]).wait_recv()
 
     def swap_kv(k, carry):
         for r in range(blocks):
@@ -306,7 +325,13 @@
             vk_in[place] = swap_halves(kv_in[place].astype(jnp.float32)).astype(jnp.bfloat16)
         return carry
 
-    lax.fori_loop(0, heads, swap_kv, 0)
+    lax.fori_loop(first_device, first_device + heads, swap_kv, 0)
+
+    def take_lower(a, carry):
+        arrival(kv_in.at[pl.ds(0, heads * blocks)], kv_recv.at[a]).wait_recv()
+        return lax.fori_loop(a * heads, (a + 1) * heads, swap_kv, carry)
+
+    lax.fori_loop(0, jnp.where(visited, 0, group), take_lower, 0)
 
     def attend(js):
         stacks = []
@@ -371,20 +396,20 @@
                 first, second = lines[2 * m : 2 * m + 1], lines[2 * m + 1 : 2 * m + 2]
                 l_out[j, m : m + 1] = jnp.where(low_line, first, swap_halves(second))
 
-    visits = (groups - 1 - group) * heads
-    opening = jnp.where((idx < heads // 2) | (visits == 0), heads, 2)
+    batch = 2
+    visits = jnp.where(visited, (groups - 1 - group) * heads, 0)
+    opening = jnp.where(visits == 0, heads, 2)
 
     def served(t):
         visiting = (t >= opening) & (t < opening + visits)
         visitor = jnp.where(visiting, t - opening, 0)
-        visitor = jnp.where(opening < heads, visitor, visits - 1 - visitor)
         own = jnp.where(t < opening, t, jnp.where(visiting, 0, heads + 1 - (t - visits)))
         target = group + jnp.where(visiting, 1 + lax.div(visitor, heads), 0)
         step = jnp.where(visiting, lax.rem(visitor, heads), own)
         return target * heads + partner(idx, step, heads)
 
     def serve(u, carry):
-        js = [served(2 * u), served(2 * u + 1)]
+        js = [served(batch * u + k) for k in range(batch)]
         for j in js:
 
             @pl.when(j != me)
@@ -407,7 +432,7 @@
 
         return carry
 
-    lax.fori_loop(0, (devices - first_device) // 2, serve, 0)
+    lax.fori_loop(0, lax.div(heads + visits, batch), serve, 0)
 
     def absent(a, carry):
         o_in[a] = jnp.zeros(o_in.shape[1:], o_in.dtype)
@@ -415,6 +440,13 @@
         return carry
 
     lax.fori_loop(group + 1, groups, absent, 0)
+
+    def partly_absent(a, carry):
+        o_in[a, :high] = jnp.zeros((high,) + o_in.shape[2:], o_in.dtype)
+        l_in[a, :high] = jnp.full((high,) + l_in.shape[2:], masked_score, jnp.float32)
+        return carry
+
+    lax.fori_loop(0, group, partly_absent, 0)
 
     def spread(body, start):
         if groups <= 2:
@@ -433,11 +465,8 @@
                 l_place = l_in.at[a, pl.ds(2 * ch, count)]
                 arrival(l_place, l_recv.at[a, ch]).wait_recv()
 
-            if i > 0:
-                take(2)
-            else:
-                pl.when(a == group)(lambda: take(1))
-                pl.when(a != group)(lambda: take(2))
+            pl.when(a == group)(lambda: take(2 if i > 0 else 1))
+            pl.when((a < group) & (2 * ch + 1 >= high))(lambda: take(min(2, high)))
             return carry
 
         lax.fori_loop(0, group + 1, take_results, 0)
@@ -500,26 +529,23 @@
         made = jnp.dot(attended[place], wo[:, columns], preferred_element_type=jnp.float32)
         stage[c, place] = made.astype(jnp.bfloat16)
 
+    for d in range(1, splits):
+        for c in range(chunks):
+            product(own_rows(d), c)
+            hop(d, c).start()
     for c in range(chunks):
-        if c < chunks - 1:
-            product(pl.ds(0, rows), c)
-        else:
-            for d in range(1, splits):
-                product(own_rows(d), c)
-        for d in range(1, splits):
-            hop(d, c).start()
-    product(own_rows(0), chunks - 1)
-    for c in range(chunks):
-        mine_ref[:, c * tile_width : (c + 1) * tile_width] = stage[c, own_rows(0)]
+        columns = slice(c * tile_width, (c + 1) * tile_width)
+        made = jnp.dot(attended[own_rows(0)], wo[:, columns], preferred_element_type=jnp.float32)
+        mine_ref[:, columns] = made.astype(jnp.bfloat16)
 
     def sent(ref, semaphore):
         arrival(ref, semaphore).wait_send()
 
-    sent(kv_out.at[pl.ds(0, heads - 1)], kv_send.at[0])
+    sent(kv_out.at[pl.ds(0, heads - 1)], kv_send.at[group])
     sent(q_out.at[pl.ds(0, heads - 1)], q_send.at[group])
 
     def sent_down(a, carry):
-        sent(q_out, q_send.at[a])
+        sent(q_out.at[pl.ds(0, heads - high)], q_send.at[a])
         return carry
 
     lax.fori_loop(0, group, sent_down, 0)
@@ -527,8 +553,13 @@
     sent(l_out.at[pl.ds(0, heads - 1)], l_send.at[group])
 
     def sent_up(a, carry):
-        sent(o_out.at[pl.ds(0, heads)], o_send.at[a])
-        sent(l_out.at[pl.ds(0, heads)], l_send.at[a])
+        sent(kv_out.at[pl.ds(0, high)], kv_send.at[a])
+
+        @pl.when(visited)
+        def _():
+            sent(o_out.at[pl.ds(0, heads)], o_send.at[a])
+            sent(l_out.at[pl.ds(0, heads)], l_send.at[a])
+
         return carry
 
     lax.fori_loop(group + 1, groups, sent_up, 0)
@@ -555,7 +586,7 @@
     bf16, f32 = jnp.bfloat16, jnp.float32
     mine, landed, logs = pl.pallas_call(
         functools.partial(layer_kernel, devices, splits),
-        in_specs=[in_vmem()] + [in_hbm()] * 5,
+        in_specs=[in_hbm()] * 6,
         out_specs=[in_vmem()] * 3,
         out_shape=[
             jax.ShapeDtypeStruct((out_rows, out_width), bf16),
@@ -569,8 +600,9 @@
             pltpu.VMEM((width, out_width), bf16),
             pltpu.VMEM((heads, blocks, BLK, LANES), bf16),
             pltpu.VMEM((heads, tiles, BLK, LANES), bf16),
-            pltpu.VMEM((heads * blocks, BLK, LANES), bf16),
-            pltpu.VMEM((heads * blocks, BLK, LANES), bf16),
+            pltpu.VMEM((devices * blocks, BLK, LANES), bf16),
+            pltpu.VMEM((devices * blocks, BLK, LANES), bf16),
+            pltpu.VMEM(chosen.shape[::-1], jnp.int32),
             pltpu.VMEM(chosen.shape[::-1], jnp.int32),
             pltpu.SMEM(chosen.shape[::-1], jnp.int32),
             pltpu.VMEM((chosen.shape[0], chosen.shape[1] * BLK), f32),
@@ -582,11 +614,11 @@
             pltpu.VMEM((heads, tiles, LANES), f32),
             pltpu.VMEM((rows, width), bf16),
             pltpu.VMEM((chunks, rows, tile_width), bf16),
-            dma((3,)),
+            dma((4,)),
             dma((pairs,)),
             dma((pairs // wide,)),
-            dma((1,)),
-            dma((1,)),
+            dma((groups,)),
+            dma((groups,)),
             dma((groups,)),
             dma((devices,)),
             dma((groups,)),
@@ -600,7 +632,7 @@
             collective_id=0, has_side_effects=True, vmem_limit_bytes=VMEM_LIMIT
         ),
         name="layer",
-    )(jnp.transpose(chosen), tokens, w_query, w_key, w_value, w_out)
+    )(pltpu.with_memory_space_constraint(jnp.transpose(chosen), pltpu.HBM), tokens, w_query, w_key, w_value, w_out)
     total = mine.astype(f32) + jnp.sum(landed.astype(f32), axis=0)
     return total.astype(bf16), logs
 

time: 41.1 us -> 39.2 us (0.954)
  Pallas kernels: 38 us -> 36.9 us
  local copies, waits for them, and re-layouts: 1.29 us -> 0.6 us
    pallas_call x1, Pallas kernels: 38 us -> 36.9 us  [local(): pl.pallas_call(functools.partial(layer_kernel, devices, splits), in_specs...]
    unnamed x3 -> x1, local copies, waits for them, and re-layouts: 1.29 us -> 0.6 us
where the time goes in v6:
time: 39.2 us; the launch traced here: 39 us
  Pallas kernels  36.9 us (94%)
  other arithmetic  0.92 us (2%)
  between operations  0.64 us (2%)
  local copies, waits for them, and re-layouts  0.6 us (2%)
    pallas_call x1, Pallas kernels, local(): pl.pallas_call(functools.partial(layer_kernel, devices, splits), in_specs...  36.9 us
    convert_element_type x1, other arithmetic, local(): return (total.astype(bf16), logs)  0.92 us

profile of v6, /device:TPU:9, one launch (start us, length us, event | category | flops | bytes accessed | tf_op | source)
XLA Modules:
  0.0 39.0 jit_solution(7925113726686261567)
XLA Ops:
  0.6 36.9 %layer.1 = (bf16[128,2048]{1,0:T(8,128)(2,1)S(1)}, bf16[1,128,2048]{2,1,0:T(8,128)(2,1)S(1)}, f32[8,256]{1,0:T(8,128)S(1)}) custom-call(s32[16,64]{1,0:T(8,128)} %bitcast.4, bf16[256,2048]{1,0:T(8,128)(2,1)} %x_ref.1, bf16[2048,512]{1,0:T(8,128)(2,1)} %wq_ref.1, bf16[2048,512]{1,0:T(8,128)(2,1)} %wk_ref.1, bf16[2048,512]{1,0:T(8,128)(2,1)} %wv_ref.1, ...), custom_call_target="tpu_custom_call" | custom-call | tf_op jit(solution)/shard_map/layer/pallas_call | solution.py:587
  37.5 0.9 %fusion = bf16[128,2048]{1,0:T(8,128)(2,1)} fusion(bf16[128,2048]{1,0:T(8,128)(2,1)S(1)} %get-tuple-element.5, bf16[1,128,2048]{2,1,0:T(8,128)(2,1)S(1)} %get-tuple-element.6), kind=kLoop, calls=%fused_computation.1 | loop fusion | flops 1048576 | bytes 1572864 | tf_op jit(solution)/shard_map/convert_element_type | solution.py:637
  38.4 0.6 %copy.9 = f32[8,256]{1,0:T(8,128)} copy(f32[8,256]{1,0:T(8,128)S(1)} %get-tuple-element.11) | data formatting | bytes 16384

commit v7 on v6

--- a/solution.py
+++ b/solution.py
@@ -58,6 +58,7 @@
     entries = chosen_ref.shape[0]
     high = heads // 2
     wide = wq.shape[2] // LANES
+    both = wkv.shape[2] // (2 * LANES)
 
     me = lax.axis_index("kv")
     tp = lax.axis_index("tp")
@@ -78,10 +79,12 @@
         return pltpu.make_async_copy(strip(wq_ref, i), target, q_load.at[i // wide])
 
     def load_k(i):
-        return pltpu.make_async_copy(strip(wk_ref, i), wkv.at[i, :, pl.ds(0, LANES)], kv_load.at[i])
+        target = wkv.at[i // both, :, pl.ds(i % both * 2 * LANES, LANES)]
+        return pltpu.make_async_copy(strip(wk_ref, i), target, kv_load.at[i // both])
 
     def load_v(i):
-        return pltpu.make_async_copy(strip(wv_ref, i), wkv.at[i, :, pl.ds(LANES, LANES)], kv_load.at[i])
+        target = wkv.at[i // both, :, pl.ds((i % both * 2 + 1) * LANES, LANES)]
+        return pltpu.make_async_copy(strip(wv_ref, i), target, kv_load.at[i // both])
 
     def loaded(ref, semaphore):
         pltpu.make_async_copy(ref, ref, semaphore).wait()
@@ -94,7 +97,7 @@
     load_x.start()
     load_lists.start()
     lowest = group == 0
-    early = 1
+    early = both
 
     def start_kv(first, last):
         for i in range(first, last):
@@ -201,16 +204,18 @@
         other = jnp.where(turn_low, pltpu.roll(part, LANES - half, 1), pltpu.roll(part, half, 1))
         return part * cos_part + other * sin_part
 
-    def make_kv(i):
-        loaded(wkv.at[i], kv_load.at[i])
-        made = jnp.dot(x[...], wkv[i], preferred_element_type=jnp.float32)
-        keys = turned(made[:, :LANES])
-        values = made[:, LANES:]
-        even = jnp.where(low_rows, keys, swap_halves(values)).astype(jnp.bfloat16)
-        odd = jnp.where(low_rows, swap_halves(keys), values).astype(jnp.bfloat16)
-        for r in range(blocks):
-            kv_out[2 * i, r] = even[r * BLK : (r + 1) * BLK]
-            kv_out[2 * i + 1, r] = odd[r * BLK : (r + 1) * BLK]
+    def make_kv(first):
+        loaded(wkv.at[first // both], kv_load.at[first // both])
+        made = jnp.dot(x[...], wkv[first // both], preferred_element_type=jnp.float32)
+        for i in range(first, first + both):
+            lane = (i - first) * 2 * LANES
+            keys = turned(made[:, lane : lane + LANES])
+            values = made[:, lane + LANES : lane + 2 * LANES]
+            even = jnp.where(low_rows, keys, swap_halves(values)).astype(jnp.bfloat16)
+            odd = jnp.where(low_rows, swap_halves(keys), values).astype(jnp.bfloat16)
+            for r in range(blocks):
+                kv_out[2 * i, r] = even[r * BLK : (r + 1) * BLK]
+                kv_out[2 * i + 1, r] = odd[r * BLK : (r + 1) * BLK]
 
     def make_q(i):
         loaded(wq.at[i // wide], q_load.at[i // wide])
@@ -279,11 +284,12 @@
         pl.semaphore_wait(barrier, devices - 1 + splits - 1)
         send_down()
 
-    for i in range(pairs):
+    for i in range(0, pairs, both):
         make_kv(i)
         if i == 0:
             pl.when(lowest)(lambda: pl.semaphore_wait(barrier, devices - 1 + splits - 1))
-        send_kv(i)
+        for e in range(both):
+            send_kv(i + e)
     send_up()
     pl.when(lowest)(make_queries)
     for i in range(pairs):
@@ -333,7 +339,7 @@
 
     lax.fori_loop(0, jnp.where(visited, 0, group), take_lower, 0)
 
-    def attend(js):
+    def attend(js, entries):
         stacks = []
         for j in js:
             for m in range(tiles):
@@ -416,7 +422,9 @@
             def _(j=j):
                 arrival(q_in.at[j], q_recv.at[j]).wait_recv()
 
-        attend(js)
+        short = functools.reduce(jnp.maximum, js) < 8 // blocks
+        pl.when(short)(lambda: attend(js, 8))
+        pl.when(jnp.logical_not(short))(lambda: attend(js, entries))
         for j in js:
 
             @pl.when(j != me)
@@ -577,7 +585,8 @@
     groups = devices // heads
     blocks = rows // BLK
     tiles = blocks // 2
-    wide = 2 if pairs % 2 == 0 else 1
+    wide = pairs
+    both = 2 if pairs % 2 == 0 else 1
 
     out_rows = rows // splits
     tile_width = min(512, out_width)
@@ -596,7 +605,7 @@
         scratch_shapes=[
             pltpu.VMEM((rows, depth), bf16),
             pltpu.VMEM((pairs // wide, depth, wide * LANES), bf16),
-            pltpu.VMEM((pairs, depth, 2 * LANES), bf16),
+            pltpu.VMEM((pairs // both, depth, both * 2 * LANES), bf16),
             pltpu.VMEM((width, out_width), bf16),
             pltpu.VMEM((heads, blocks, BLK, LANES), bf16),
             pltpu.VMEM((heads, tiles, BLK, LANES), bf16),
@@ -615,7 +624,7 @@
             pltpu.VMEM((rows, width), bf16),
             pltpu.VMEM((chunks, rows, tile_width), bf16),
             dma((4,)),
-            dma((pairs,)),
+            dma((pairs // both,)),
             dma((pairs // wide,)),
             dma((groups,)),
             dma((groups,)),

time: 39.2 us -> 38.4 us (0.980)
  Pallas kernels: 36.9 us -> 36.1 us
    pallas_call x1, Pallas kernels: 36.9 us -> 36.1 us  [local(): pl.pallas_call(functools.partial(layer_kernel, devices, splits), in_specs...]
where the time goes in v7:
time: 38.4 us; the launch traced here: 38.3 us
  Pallas kernels  36.1 us (94%)
  other arithmetic  0.92 us (2%)
  between operations  0.64 us (2%)
  local copies, waits for them, and re-layouts  0.6 us (2%)
    pallas_call x1, Pallas kernels, local(): pl.pallas_call(functools.partial(layer_kernel, devices, splits), in_specs...  36.1 us
    convert_element_type x1, other arithmetic, local(): return (total.astype(bf16), logs)  0.92 us

profile of v7, /device:TPU:9, one launch (start us, length us, event | category | flops | bytes accessed | tf_op | source)
XLA Modules:
  0.0 38.3 jit_solution(6879212689631242724)
XLA Ops:
  0.6 36.1 %layer.1 = (bf16[128,2048]{1,0:T(8,128)(2,1)S(1)}, bf16[1,128,2048]{2,1,0:T(8,128)(2,1)S(1)}, f32[8,256]{1,0:T(8,128)S(1)}) custom-call(s32[16,64]{1,0:T(8,128)} %bitcast.4, bf16[256,2048]{1,0:T(8,128)(2,1)} %x_ref.1, bf16[2048,512]{1,0:T(8,128)(2,1)} %wq_ref.1, bf16[2048,512]{1,0:T(8,128)(2,1)} %wk_ref.1, bf16[2048,512]{1,0:T(8,128)(2,1)} %wv_ref.1, ...), custom_call_target="tpu_custom_call" | custom-call | tf_op jit(solution)/shard_map/layer/pallas_call | solution.py:596
  36.7 0.9 %fusion = bf16[128,2048]{1,0:T(8,128)(2,1)} fusion(bf16[128,2048]{1,0:T(8,128)(2,1)S(1)} %get-tuple-element.5, bf16[1,128,2048]{2,1,0:T(8,128)(2,1)S(1)} %get-tuple-element.6), kind=kLoop, calls=%fused_computation.1 | loop fusion | flops 1048576 | bytes 1572864 | tf_op jit(solution)/shard_map/convert_element_type | solution.py:646
  37.7 0.6 %copy.9 = f32[8,256]{1,0:T(8,128)} copy(f32[8,256]{1,0:T(8,128)S(1)} %get-tuple-element.11) | data formatting | bytes 16384

commit v8 on v7

--- a/solution.py
+++ b/solution.py
@@ -12,7 +12,7 @@
 BLK = 64
 LANES = 128
 VMEM_LIMIT = 55_000_000
-AHEAD = 2
+AHEAD = 3
 LOG2_E = float(np.log2(np.e))
 
 rotary_base = 500000.0

time: 38.4 us -> 37.2 us (0.969)
  Pallas kernels: 36.1 us -> 34.9 us
    pallas_call x1, Pallas kernels: 36.1 us -> 34.9 us  [local(): pl.pallas_call(functools.partial(layer_kernel, devices, splits), in_specs...]
where the time goes in v8:
time: 37.2 us; the launch traced here: 37 us
  Pallas kernels  34.9 us (94%)
  other arithmetic  0.92 us (2%)
  between operations  0.64 us (2%)
  local copies, waits for them, and re-layouts  0.6 us (2%)
    pallas_call x1, Pallas kernels, local(): pl.pallas_call(functools.partial(layer_kernel, devices, splits), in_specs...  34.9 us
    convert_element_type x1, other arithmetic, local(): return (total.astype(bf16), logs)  0.92 us

profile of v8, /device:TPU:9, one launch (start us, length us, event | category | flops | bytes accessed | tf_op | source)
XLA Modules:
  0.0 37.0 jit_solution(10069142902659790869)
XLA Ops:
  0.6 34.9 %layer.1 = (bf16[128,2048]{1,0:T(8,128)(2,1)S(1)}, bf16[1,128,2048]{2,1,0:T(8,128)(2,1)S(1)}, f32[8,256]{1,0:T(8,128)S(1)}) custom-call(s32[16,64]{1,0:T(8,128)} %bitcast.4, bf16[256,2048]{1,0:T(8,128)(2,1)} %x_ref.1, bf16[2048,512]{1,0:T(8,128)(2,1)} %wq_ref.1, bf16[2048,512]{1,0:T(8,128)(2,1)} %wk_ref.1, bf16[2048,512]{1,0:T(8,128)(2,1)} %wv_ref.1, ...), custom_call_target="tpu_custom_call" | custom-call | tf_op jit(solution)/shard_map/layer/pallas_call | solution.py:596
  35.5 0.9 %fusion = bf16[128,2048]{1,0:T(8,128)(2,1)} fusion(bf16[128,2048]{1,0:T(8,128)(2,1)S(1)} %get-tuple-element.5, bf16[1,128,2048]{2,1,0:T(8,128)(2,1)S(1)} %get-tuple-element.6), kind=kLoop, calls=%fused_computation.1 | loop fusion | flops 1048576 | bytes 1572864 | tf_op jit(solution)/shard_map/convert_element_type | solution.py:646
  36.4 0.6 %copy.9 = f32[8,256]{1,0:T(8,128)} copy(f32[8,256]{1,0:T(8,128)S(1)} %get-tuple-element.11) | data formatting | bytes 16384
